TPU v7x, 256 devices: a 4x2x16 block of a 4x16x16 slice. The times are simulated.
256 devices in a mesh: grp: 2 (over y), tp: 16 (over z), dp: 8 (over x, core).
Axes of the slice: x: 4, y: 2, z: 16, core: 2. Of those that a mesh axis runs over, the one named last changes fastest.
The devices are a block of a 4x16x16 slice.
Arguments:
- skip_path_activations: bfloat16 [256, 8, 4096], P('grp', None, 'dp'), parts along dimension 0
- novel_lengths_per_sequence: int32 [256], P(('grp', 'dp')), parts along dimension 0, may hold values from 1 to 8, 512 in all
- input_normalizer_scales: bfloat16 [2, 4096], P(None, 'dp'), may hold values from 0.099609375 to 1.8984375
- question_projector: bfloat16 [2, 4096, 2048], P(None, 'dp', 'tp'), may hold values from -0.09375 to 0.09375
- lookup_projector: bfloat16 [2, 4096, 2048], P(None, 'dp', 'tp'), may hold values from -0.09375 to 0.09375
- payload_projector: bfloat16 [2, 4096, 4096], P(None, 'dp', 'tp'), may hold values from -0.09375 to 0.09375
- emitted_valve_projector: bfloat16 [2, 4096, 4096], P(None, 'dp', 'tp'), may hold values from -0.09375 to 0.09375
- keeping_valve_projector: bfloat16 [2, 4096, 2048], P(None, 'dp', 'tp'), may hold values from -0.09375 to 0.09375
- keeping_valve_shift: float32 [2, 2048], P(None, 'tp'), may hold values from -3 to 6
- additional_dwindle_exponent: float32 [256, 8, 16], P(('grp', 'dp'), None, 'tp'), parts along dimension 0, may hold values from -0.7 to 0
- headwise_normalizer_scales: bfloat16 [2, 256], replicated, may hold values from 0.099609375 to 1.8984375
- closing_projector: bfloat16 [2, 4096, 4096], P(None, 'tp', 'dp'), may hold values from -0.1875 to 0.1875
- earlier_recurrence_grid: float32 [2, 256, 16, 128, 256], P(None, ('grp', 'dp'), 'tp'), parts along dimension 1, may hold values from -6 to 6
Outputs:
- stream_out: bfloat16 [256, 8, 4096], P('grp', None, 'dp'), parts along dimension 0
- state_out: float32 [2, 256, 16, 128, 256], P(None, ('grp', 'dp'), 'tp'), parts along dimension 1
There are 2 independent parts, one for each index of `grp`. A program takes and returns all parts, laid end to end along the dimension named above; an argument that names none is the same for every part. Nothing has to cross between parts.
Inputs may be any that keep to these rules, and one draw needn't show every extreme that they name: `novel_lengths_per_sequence`: each sequence has 1 to 8 live token slots, the first ones; some sequence has 8. In each group the live slots of its 128 sequences add up to half of 128 times 8.
All inputs are finite; a program needn't handle non-finite values.
Results may differ from a plain program's by a relative error of at most 0.024.
Values may be sent and summed in bfloat16 or wider, within the bound.
No kernel may reach another device: no remote copies, remote signals or barrier semaphores. Data moves between devices by JAX's collectives and lax.ppermute only.
A program may use at most 64 MiB of HBM per device.

v0:
```python
import functools

import jax
import jax.numpy as jnp
from jax import lax
from jax.experimental import pallas as pl
from jax.experimental.pallas import tpu as pltpu
from jax.sharding import PartitionSpec as P


EPS = 1e-06
TAU = 16.0
BF = jnp.bfloat16
F32 = jnp.float32
VMEM_LIMIT = 8 * 1024 * 1024
ROUNDS = 4
SIDE = 128


def dot(a, b):
    return jnp.dot(a, b, preferred_element_type=F32)


def params(*semantics):
    return pltpu.CompilerParams(vmem_limit_bytes=VMEM_LIMIT, dimension_semantics=semantics or None)


def row_of(ref, layer):
    row = ref[0:1, :]
    for i in range(1, ref.shape[0]):
        row = jnp.where(layer == i, ref[i : i + 1, :], row)
    return row


def in_hbm(x):
    return pltpu.with_memory_space_constraint(x, pltpu.MemorySpace.HBM)


def whole(shape):
    return pl.BlockSpec(shape, lambda *_: (0,) * len(shape))


def project(layer, x, gain_ref, w_refs, out_ref, lens_col):
    blocks, _, rows, _ = out_ref.shape
    xf = x.astype(F32)
    gain = row_of(gain_ref, layer).astype(F32)
    scaled = jnp.clip(xf * gain, -1e30, 1e30).astype(BF)

    def put(half, at, value):
        for j in range(blocks):
            out_ref[j, half, :, at : at + value.shape[1]] = value[j * rows : (j + 1) * rows].astype(BF)

    ends = []
    for half, group in enumerate((w_refs[:3], w_refs[3:])):
        at = 0
        for w in group:
            put(half, at, dot(scaled, w[0]))
            at += w.shape[-1]
        ends.append(at)
    squares = jnp.sum(xf * xf, axis=1, keepdims=True)
    high = squares.astype(BF).astype(F32)
    low = jnp.where(jnp.abs(high) < 3.0e38, squares - high, 0.0)
    lane = lax.broadcasted_iota(jnp.int32, (x.shape[0], SIDE), 1)
    side = jnp.where(lane == 0, high, jnp.where(lane == 1, low, 0.0))
    if lens_col is not None:
        side = jnp.where(lane == 2, lens_col, side)
    put(1, ends[1], side)


def project_first(layer, local_seqs, meta, lens, x0, x1, gain_ref, wq, wk, wv, wr, wf, out_ref):
    x = jnp.concatenate([x0[...], x1[...]], axis=0)
    rows = x0.shape[0]
    row = lax.broadcasted_iota(jnp.int32, (rows, SIDE), 0) - meta[9] * local_seqs
    lens_col = jnp.zeros((rows, SIDE), F32)
    for s in range(local_seqs):
        lens_col = jnp.where(row == s, lens[s].astype(F32), lens_col)
    lens_col = jnp.concatenate([lens_col] * 2, axis=0)
    project(layer, x, gain_ref, (wq, wk, wv, wr, wf), out_ref, lens_col)


def piece_ids(meta, shape, offset):
    span = shape[1] // ROUNDS
    lane = lax.broadcasted_iota(jnp.int32, shape, 1)
    block = lax.rem(meta[8] + offset + ROUNDS, ROUNDS) + ROUNDS * (lane // span)
    return (block * span + lax.rem(lane, span)).astype(F32)


def expand(meta, where_rows, pieces):
    own, plus, minus, far = pieces
    rows = where_rows[0].shape[1]
    place = jnp.concatenate(
        [jnp.transpose(jnp.broadcast_to(r, (rows, rows)))[:, :1] for r in where_rows], axis=0
    )
    at = jnp.broadcast_to(place, (place.shape[0], own.shape[0]))

    def chosen(offset):
        return (at == piece_ids(meta, at.shape, offset)).astype(F32).astype(BF)

    x = dot(chosen(0), own[...]) + dot(chosen(1), plus[...]) + dot(chosen(-1), minus[...])
    return x + dot(chosen(2), far[...]), place


def project_next(layer, meta, where_ref, *refs):
    *pieces, gain_ref, wq, wk, wv, wr, wf, out_ref = refs
    first = 2 * pl.program_id(0)
    rows = [where_ref[pl.ds(meta[first + j], 1), :] for j in range(2)]
    x, _ = expand(meta, rows, pieces)
    project(layer, x, gain_ref, (wq, wk, wv, wr, wf), out_ref, None)


def finish(blocks, meta, where_ref, *refs):
    *pieces, x_ref, out_ref = refs
    first = pl.program_id(0) * blocks
    rows = [where_ref[pl.ds(first + j, 1), :] for j in range(blocks)]
    live, place = expand(meta, rows, pieces)
    out_ref[...] = jnp.where(place < 0, x_ref[...].astype(F32), live).astype(BF)


def weight_spec(layer, w):
    return pl.BlockSpec((1, w.shape[1], w.shape[2]), lambda *_: (layer, 0, 0))


def projected(weights, rows, blocks):
    cols = sum(w.shape[2] for w in weights[:3])
    assert cols == sum(w.shape[2] for w in weights[3:]) + SIDE
    return jax.ShapeDtypeStruct((blocks, 2, rows, cols), BF)


def call_project_first(layer, meta, lens, x, gain, weights, blocks):
    rows, width = x.shape[0] // (2 * blocks), x.shape[1]
    out = projected(weights, rows, blocks)

    def block_of(j):
        return pl.BlockSpec((rows, width), lambda i, meta, lens: (meta[2 * i + j], 0))

    return pl.pallas_call(
        functools.partial(project_first, layer, lens.shape[0]),
        grid_spec=pltpu.PrefetchScalarGridSpec(
            num_scalar_prefetch=2,
            grid=(blocks // 2,),
            in_specs=[
                *(block_of(j) for j in range(2)),
                whole(gain.shape),
                *(weight_spec(layer, w) for w in weights),
            ],
            out_specs=pl.BlockSpec((2, *out.shape[1:]), lambda i, *_: (i, 0, 0, 0)),
        ),
        out_shape=out,
        compiler_params=params("arbitrary"),
        name="project_first",
    )(meta, lens, *([in_hbm(x)] * 2), in_hbm(gain), *(in_hbm(w) for w in weights))


def piece_specs(pieces):
    return [whole(p.shape) for p in pieces]


def call_project_next(layer, meta, where, pieces, gain, weights, blocks):
    out = projected(weights, where.shape[1], blocks)
    return pl.pallas_call(
        functools.partial(project_next, layer),
        grid_spec=pltpu.PrefetchScalarGridSpec(
            num_scalar_prefetch=1,
            grid=(blocks // 2,),
            in_specs=[
                whole(where.shape),
                *piece_specs(pieces),
                whole(gain.shape),
                *(weight_spec(layer, w) for w in weights),
            ],
            out_specs=pl.BlockSpec((2, *out.shape[1:]), lambda i, *_: (i, 0, 0, 0)),
        ),
        out_shape=out,
        compiler_params=params("arbitrary"),
        name="project_next",
    )(meta, where, *pieces, gain, *weights)


def call_finish(meta, where, pieces, x):
    owners, rows = where.shape
    blocks = owners // 2
    return pl.pallas_call(
        functools.partial(finish, blocks),
        grid_spec=pltpu.PrefetchScalarGridSpec(
            num_scalar_prefetch=1,
            grid=(owners // blocks,),
            in_specs=[
                whole(where.shape),
                *piece_specs(pieces),
                pl.BlockSpec((blocks * rows, x.shape[1]), lambda i, *_: (i, 0)),
            ],
            out_specs=pl.BlockSpec((blocks * rows, x.shape[1]), lambda i, *_: (i, 0)),
        ),
        out_shape=jax.ShapeDtypeStruct(x.shape, BF),
        compiler_params=params("arbitrary"),
        name="finish",
    )(meta, where, *pieces, x)


def recur(full_width, steps, meta, lens, *refs):
    layer = meta[10]
    (mine, core, up, down, shift_ref, extra_ref, hs_ref, state), rest = refs[:8], refs[8:]
    g_ref, wk_ref, v_ref, end_ref, side_ref = rest
    seqs, key_dim, value_dim = state.shape
    rows = seqs * steps
    sum_a, sum_b = [
        (mine[0, h].astype(F32) + core[0, h].astype(F32)) + (up[h].astype(F32) + down[h].astype(F32))
        for h in range(2)
    ]
    at = value_dim + key_dim
    side = sum_b[:, at : at + SIDE]
    squares = side[:, 0:1] + side[:, 1:2]
    rms = lax.rsqrt(squares / full_width + EPS)
    q = sum_a[:, :key_dim] * (rms * key_dim ** (-0.5))
    k = sum_a[:, key_dim : 2 * key_dim] * rms
    v = sum_a[:, 2 * key_dim :] * rms
    r = sum_b[:, :value_dim] * rms
    f = sum_b[:, value_dim:at] * rms

    row = lax.broadcasted_iota(jnp.int32, (rows, key_dim), 0)
    own_len = jnp.zeros((rows, key_dim), jnp.int32)
    for s in range(seqs):
        own_len = jnp.where(row // steps == s, lens[s], own_len)
    live = jnp.where(lax.rem(row, steps) < own_len, 1.0, 0.0)
    logits = f + row_of(shift_ref, layer)
    log_sig = jnp.minimum(logits, 0.0) - jnp.log(1.0 + jnp.exp(-jnp.abs(logits)))
    fade = (log_sig / TAU + extra_ref[...]) * live
    k = k * live

    def by_seq(x):
        return x.reshape(seqs, steps, x.shape[1])

    q3, k3, v3, fade3 = by_seq(q), by_seq(k), by_seq(v), by_seq(fade)
    slot = lax.broadcasted_iota(jnp.int32, (seqs, steps, key_dim), 1)
    total = jnp.zeros_like(fade3)
    for j in range(steps):
        total = total + jnp.where(slot >= j, fade3[:, j : j + 1, :], 0.0)
    out = jnp.zeros_like(v3)
    for j in range(steps):
        apart = jnp.where(slot >= j, total - total[:, j : j + 1, :], -1e30)
        score = jnp.sum(q3 * k3[:, j : j + 1, :] * jnp.exp(apart), axis=-1, keepdims=True)
        out = out + score * v3[:, j : j + 1, :]
    last = total[:, steps - 1 : steps, :]
    wk_ref[...] = (k3 * jnp.exp(last - total)).reshape(rows, key_dim).astype(BF)
    v_ref[...] = v.astype(BF)
    end_ref[...] = jnp.exp(last)
    side_ref[...] = side
    weighted = (q3 * jnp.exp(total)).reshape(rows, key_dim).astype(BF)
    carried = [
        dot(weighted[s * steps : (s + 1) * steps], state[s].astype(BF)) for s in range(seqs)
    ]
    out = out.reshape(rows, value_dim) + jnp.concatenate(carried, axis=0)
    scale = lax.rsqrt(jnp.mean(out * out, axis=-1, keepdims=True) + EPS)
    silu = r / (1.0 + jnp.exp(-r))
    g_ref[...] = (out * scale * row_of(hs_ref, layer).astype(F32) * silu * live[:, :1]).astype(BF)


def call_recur(meta, full_width, lens, parts, shift, extra, head_scale, state, steps):
    seqs, key_dim, value_dim = state.shape
    rows = seqs * steps
    mine, _, up, down = parts
    first = pl.BlockSpec((1, *mine.shape[1:]), lambda *_: (0, 0, 0, 0))
    out_shape = [
        jax.ShapeDtypeStruct((rows, value_dim), BF),
        jax.ShapeDtypeStruct((rows, key_dim), BF),
        jax.ShapeDtypeStruct((rows, value_dim), BF),
        jax.ShapeDtypeStruct((seqs, 1, key_dim), F32),
        jax.ShapeDtypeStruct((rows, SIDE), F32),
    ]
    return pl.pallas_call(
        functools.partial(recur, full_width, steps),
        grid_spec=pltpu.PrefetchScalarGridSpec(
            num_scalar_prefetch=2,
            grid=(1,),
            in_specs=[
                first,
                first,
                whole(up.shape),
                whole(down.shape),
                whole(shift.shape),
                whole((rows, 1)),
                whole(head_scale.shape),
                whole(state.shape),
            ],
            out_specs=[whole(o.shape) for o in out_shape],
        ),
        out_shape=out_shape,
        compiler_params=params("arbitrary"),
        name="recur",
    )(meta, lens, *parts, shift, extra, head_scale, state)


def plan(steps, side_ref, where_ref):
    side = side_ref[...]
    rows = where_ref.shape[1]
    owners = where_ref.shape[0]
    n = side.shape[0]
    lens_all = jnp.broadcast_to(side[:, 2:3], side.shape).astype(BF)
    seq_of = lax.broadcasted_iota(jnp.int32, (n, owners * rows), 1) // steps
    seq = lax.broadcasted_iota(jnp.int32, (n, owners * rows), 0)
    before = (seq < seq_of).astype(F32).astype(BF)
    same = (seq == seq_of).astype(F32).astype(BF)
    over = (((0,), (0,)), ((), ()))
    start = lax.dot_general(lens_all, before, over, preferred_element_type=F32)[:8]
    length = lax.dot_general(lens_all, same, over, preferred_element_type=F32)[:8]
    t = lax.rem(lax.broadcasted_iota(jnp.int32, start.shape, 1), steps).astype(F32)
    spot = jnp.where(t < length, start + t, -1.0)
    for d in range(owners):
        where_ref[d : d + 1, :] = spot[:1, d * rows : (d + 1) * rows]


def call_plan(steps, owners, side):
    out = jax.ShapeDtypeStruct((owners, side.shape[0]), F32)
    return pl.pallas_call(
        functools.partial(plan, steps),
        grid=(1,),
        in_specs=[whole(side.shape)],
        out_specs=whole(out.shape),
        out_shape=out,
        compiler_params=params("arbitrary"),
        name="plan",
    )(side)


def load(layer, after_ref, state_hbm, out_ref, sem):
    copy = pltpu.make_async_copy(state_hbm.at[layer], out_ref, sem)
    copy.start()
    copy.wait()


def call_load(layer, after, state):
    return pl.pallas_call(
        functools.partial(load, layer),
        grid=(1,),
        in_specs=[whole(after.shape), pl.BlockSpec(memory_space=pltpu.MemorySpace.HBM)],
        out_specs=pl.BlockSpec(memory_space=pltpu.MemorySpace.VMEM),
        out_shape=pltpu.VMEM(state.shape[1:], F32),
        scratch_shapes=[pltpu.SemaphoreType.DMA],
        compiler_params=params("arbitrary"),
        name="load_state",
    )(after, in_hbm(state))


def update(steps, wk_ref, v_ref, end_ref, state_ref, *refs):
    out_ref = refs[-1]
    for s in range(state_ref.shape[0]):
        keys = wk_ref[s * steps : (s + 1) * steps, :]
        values = v_ref[s * steps : (s + 1) * steps, :]
        fresh = lax.dot_general(keys, values, (((0,), (0,)), ((), ())), preferred_element_type=F32)
        end = end_ref[s]
        keep = jnp.transpose(jnp.broadcast_to(end, (end.shape[1], end.shape[1])))[:, :1]
        out_ref[0, s] = keep * state_ref[s] + fresh


def call_update(layer, layers, steps, wk, v, end, state, previous):
    seqs, key_dim, value_dim = state.shape
    step_seqs = 4
    block = pl.BlockSpec((1, step_seqs, key_dim, value_dim), lambda i: (layer, i, 0, 0))
    operands = [wk, v, end, state]
    in_specs = [
        pl.BlockSpec((step_seqs * steps, key_dim), lambda i: (i, 0)),
        pl.BlockSpec((step_seqs * steps, value_dim), lambda i: (i, 0)),
        pl.BlockSpec((step_seqs, 1, key_dim), lambda i: (i, 0, 0)),
        pl.BlockSpec((step_seqs, key_dim, value_dim), lambda i: (i, 0, 0)),
    ]
    alias = {}
    if previous is not None:
        operands.append(previous)
        in_specs.append(pl.BlockSpec(memory_space=pl.ANY))
        alias = {4: 0}
    return pl.pallas_call(
        functools.partial(update, steps),
        grid=(seqs // step_seqs,),
        in_specs=in_specs,
        out_specs=block,
        out_shape=jax.ShapeDtypeStruct((layers, *state.shape), F32),
        input_output_aliases=alias,
        compiler_params=params("arbitrary"),
        name="update_state",
    )(*operands)


def target_ids(meta, shape, span):
    row = lax.broadcasted_iota(jnp.int32, shape, 0)
    block = lax.rem(meta[8] + row // (ROUNDS * span), ROUNDS) + ROUNDS * lax.rem(row // span, ROUNDS)
    return (block * span + lax.rem(row, span)).astype(F32)


def close(tp, meta, where_ref, *refs):
    *g_refs, c_ref, own, plus, minus, far = refs
    rows = where_ref.shape[1]
    n = own.shape[0]
    count = n * ROUNDS
    span = count // tp
    ids = target_ids(meta, (count, rows), span)
    gathered = jnp.zeros((count, c_ref.shape[1]), F32)
    i = 0
    for g in g_refs:
        for b in range(g.shape[0]):
            chosen = (ids == where_ref[pl.ds(meta[16 + i], 1), :]).astype(F32).astype(BF)
            gathered = gathered + dot(chosen, g[b])
            i += 1
    y = dot(gathered.astype(BF), c_ref[0])
    own[...] = y[:n]
    plus[...] = y[n : 2 * n].astype(BF)
    far[...] = y[2 * n : 3 * n].astype(BF)
    minus[...] = y[3 * n :].astype(BF)


def call_close(tp, meta, where, gs, closing, live_rows):
    width = closing.shape[2]
    n = live_rows // ROUNDS
    out_shape = [
        jax.ShapeDtypeStruct((n, width), F32),
        jax.ShapeDtypeStruct((n, width), BF),
        jax.ShapeDtypeStruct((n, width), BF),
        jax.ShapeDtypeStruct((n, width), BF),
    ]
    return pl.pallas_call(
        functools.partial(close, tp),
        grid_spec=pltpu.PrefetchScalarGridSpec(
            num_scalar_prefetch=1,
            grid=(1,),
            in_specs=[
                whole(where.shape),
                *(whole(g.shape) for g in gs),
                pl.BlockSpec((1, *closing.shape[1:]), lambda i, meta: (meta[10], 0, 0)),
            ],
            out_specs=[whole(o.shape) for o in out_shape],
        ),
        out_shape=out_shape,
        compiler_params=params("arbitrary"),
        name="close",
    )(meta, where, *gs, closing)


def own_rows(span, meta, where_ref, x_ref, out_ref):
    rows = where_ref.shape[1]
    ids = target_ids(meta, (out_ref.shape[0], rows), span)
    total = jnp.zeros(out_ref.shape, F32)
    for d in range(where_ref.shape[0]):
        chosen = (ids == where_ref[d : d + 1, :]).astype(F32).astype(BF)
        total = total + dot(chosen, x_ref[d * rows : (d + 1) * rows, :])
    out_ref[...] = total.astype(BF)


def call_own_rows(tp, meta, where, x, live_rows):
    out = jax.ShapeDtypeStruct((live_rows // ROUNDS, x.shape[1]), BF)
    return pl.pallas_call(
        functools.partial(own_rows, live_rows // tp),
        grid_spec=pltpu.PrefetchScalarGridSpec(
            num_scalar_prefetch=1,
            grid=(1,),
            in_specs=[whole(where.shape), whole(x.shape)],
            out_specs=whole(out.shape),
        ),
        out_shape=out,
        compiler_params=params("arbitrary"),
        name="own_rows",
    )(meta, where, x)


def to_chip(x, step):
    n = lax.axis_size("dp")
    return lax.ppermute(x, "dp", [(d, (d + 2 * step) % n) for d in range(n)])


def to_core(x):
    n = lax.axis_size("dp")
    return lax.ppermute(x, "dp", [(d, d ^ 1) for d in range(n)])


def along(x, step):
    n = lax.axis_size("tp")
    return lax.ppermute(x, "tp", [(i, (i + step) % n) for i in range(n)])


def across(x, flip):
    n = lax.axis_size("tp")
    return lax.ppermute(x, "tp", [(i, ROUNDS * ((i // ROUNDS) ^ flip) + i % ROUNDS) for i in range(n)])


def dp_sum(send, mine, fetch):
    core = to_core(send)

    def both(j, h):
        return mine[j, h].astype(F32) + core[j, h].astype(F32)

    far_a = to_chip(both(2, 0).astype(BF), 1)
    far_b = to_chip(both(2, 1).astype(BF), -1)
    up = jnp.stack([both(1, 0) + far_a.astype(F32), both(1, 1)]).astype(BF)
    down = jnp.stack([both(3, 0), both(3, 1) + far_b.astype(F32)]).astype(BF)
    state = fetch(far_b[:8, :128])
    up, down = to_chip(up, 1), to_chip(down, -1)
    up, state = lax.optimization_barrier((up, state))
    return (mine, core, up, down), state


def dp_gather(g):
    n = lax.axis_size("dp")
    far = to_chip(g, -2)
    near = jnp.stack([g, to_chip(g, -1), far, to_chip(g, 1)])
    pairs = [[d, d + 1] for d in range(0, n, 2)]
    return lax.all_gather(near, "dp", axis_index_groups=pairs, tiled=True)


def tp_sum(parts, x_own, update):
    own, plus, minus, far = parts
    total = own + along(far, 2).astype(F32)
    total = total + along(plus, 1).astype(F32) + along(minus, -1).astype(F32)
    total = total.astype(BF)
    half = total.shape[1] // 2
    left, right = total[:, :half], total[:, half:]

    def add(a, b):
        return (a.astype(F32) + b.astype(F32)).astype(BF)

    x_own, total, state = update(x_own, total)
    got_left, got_right = across(left, 1), across(right, 3)
    got_left, x_own = lax.optimization_barrier((got_left, x_own))
    left, right = add(left, got_left), add(right, got_right)
    got_left, got_right = across(left, 3), across(right, 1)
    mixed = jnp.concatenate(
        [left.astype(F32) + got_left.astype(F32), right.astype(F32) + got_right.astype(F32)], axis=1
    )
    return (x_own.astype(F32) + mixed).astype(BF), state


def tp_gather(own):
    far = along(own, -2)
    plus = along(own, -1)
    minus = along(own, 1)
    return own, plus, minus, far


def shards(
    skip_path_activations,
    novel_lengths_per_sequence,
    input_normalizer_scales,
    question_projector,
    lookup_projector,
    payload_projector,
    emitted_valve_projector,
    keeping_valve_projector,
    keeping_valve_shift,
    additional_dwindle_exponent,
    headwise_normalizer_scales,
    closing_projector,
    earlier_recurrence_grid,
):
    streams, steps, width = skip_path_activations.shape
    dp, tp = lax.axis_size("dp"), lax.axis_size("tp")
    chips = dp // 2
    full_width = width * dp
    live_rows = streams * steps // 2
    x = skip_path_activations.reshape(streams * steps, width)
    lens = novel_lengths_per_sequence
    gain = input_normalizer_scales
    weights = (
        question_projector,
        lookup_projector,
        payload_projector,
        emitted_valve_projector,
        keeping_valve_projector,
    )
    layers, seqs, heads, key_dim, value_dim = earlier_recurrence_grid.shape
    state = earlier_recurrence_grid.reshape(layers, seqs * heads, key_dim, value_dim)
    extra = additional_dwindle_exponent.reshape(seqs * steps, 1)

    me = lax.axis_index("dp")
    slot = lax.iota(jnp.int32, 32)
    side_core = (slot // chips) % 2
    owner = 2 * ((me // 2 + slot) % chips) + jnp.where(slot < 16, (me % 2) ^ side_core, side_core)
    meta = jnp.where(slot == 8, lax.axis_index("tp"), jnp.where(slot == 9, me, owner)).astype(jnp.int32)
    metas = [jnp.where(slot == 10, layer, meta) for layer in range(layers)]
    other = meta ^ (slot < 2 * chips)

    new_state = None
    where = x_own = pieces = None
    for layer in range(layers):
        if layer == 0:
            run = lambda order: call_project_first(layer, order, in_hbm(lens), x, gain, weights, chips)
        else:
            run = lambda order: call_project_next(layer, order, where, pieces, gain, weights, chips)
        send, mine = [run(order) for order in (other, metas[layer])]
        parts, held = dp_sum(send, mine, lambda after: call_load(layer, after, state))
        g, wk, v, end, side = call_recur(
            metas[layer], full_width, lens, parts, keeping_valve_shift, extra,
            headwise_normalizer_scales, held, steps,
        )
        if layer == 0:
            where = call_plan(steps, dp, side)
            x_own = call_own_rows(tp, meta, where, x, live_rows)
        sums = call_close(tp, metas[layer], where, [dp_gather(g)], closing_projector, live_rows)

        def update(own, total):
            total, keys = lax.optimization_barrier((total, wk))
            fresh = call_update(layer, layers, steps, keys, v, end, held, new_state)
            own, fresh = lax.optimization_barrier((own, fresh))
            return own, total, fresh

        x_own, new_state = tp_sum(sums, x_own, update)
        pieces = tp_gather(x_own)
    stream = call_finish(meta, where, pieces, x)
    return (
        stream.reshape(streams, steps, width),
        new_state.reshape(earlier_recurrence_grid.shape),
    )


def solution(mesh):
    in_specs = (
        P("grp", None, "dp"),
        P(("grp", "dp")),
        P(None, "dp"),
        P(None, "dp", "tp"),
        P(None, "dp", "tp"),
        P(None, "dp", "tp"),
        P(None, "dp", "tp"),
        P(None, "dp", "tp"),
        P(None, "tp"),
        P(("grp", "dp"), None, "tp"),
        P(),
        P(None, "tp", "dp"),
        P(None, ("grp", "dp"), "tp", None, None),
    )
    out_specs = (P("grp", None, "dp"), P(None, ("grp", "dp"), "tp", None, None))
    return jax.shard_map(shards, mesh=mesh, in_specs=in_specs, out_specs=out_specs, check_vma=False)
```

profile of v0, /device:TPU:33, one launch (start us, length us, event | category | flops | bytes accessed | tf_op | source)
XLA Modules:
  0.0 203.1 jit_solution(13279522742225885956)
XLA Ops:
  0.7 3.1 %project_first.3 = bf16[4,2,128,512]{3,2,1,0:T(8,128)(2,1)S(1)} custom-call(s32[32]{0:T(128)S(1)} %get-tuple-element.92.meta, s32[16]{0:T(128)} %lens.7, bf16[1024,512]{1,0:T(8,128)(2,1)} %bitcast.64, bf16[1024,512]{1,0:T(8,128)(2,1)} %bitcast.65, bf16[2,512]{1,0:T(2,128)(2,1)} %refs_4_.6, bf16[2,512,128]{2,1,0:T(8,128)(2,1)} %refs_5_.3, ...), custom_call_target="tpu_custom_call" | custom-call | tf_op jit(solution)/shard_map/project_first/pallas_call | solution.py:136
  3.8 20.5 %collective-permute-start = (bf16[4,2,128,512]{3,2,1,0:T(8,128)(2,1)S(1)}, bf16[4,2,128,512]{3,2,1,0:T(8,128)(2,1)S(1)}, u32[]{:S(2)}, u32[]{:S(2)}) collective-permute-start(bf16[4,2,128,512]{3,2,1,0:T(8,128)(2,1)S(1)} %project_first.3), channel_id=1, source_target_pairs={{0,1},{1,0},{2,3},{3,2},{4,5},{5,4},{6,7},{7,6},{8,9},{9,8},{10,11... | collective-permute-start | bytes 3145736 | tf_op jit(solution)/shard_map/ppermute | solution.py:470
  24.3 3.2 %project_first.2.refs_0_ = bf16[4,2,128,512]{3,2,1,0:T(8,128)(2,1)S(1)} custom-call(s32[32]{0:T(128)S(1)} %get-tuple-element.93.meta, s32[16]{0:T(128)} %lens.7, bf16[1024,512]{1,0:T(8,128)(2,1)} %bitcast.66, bf16[1024,512]{1,0:T(8,128)(2,1)} %bitcast.67, bf16[2,512]{1,0:T(2,128)(2,1)} %refs_4_.6, bf16[2,512,128]{2,1,0:T(8,128)(2,1)} %refs_5_.3, ...), custom_call_target="tpu_custom_call" | custom-call | tf_op jit(solution)/shard_map/project_first/pallas_call | solution.py:136
  27.9 1.4 collective-permute-start.1
  29.3 3.7 %collective-permute-done.3 = bf16[128,512]{1,0:T(8,128)(2,1)S(1)} collective-permute-done((bf16[128,512]{1,0:T(8,128)(2,1)S(1)}, bf16[128,512]{1,0:T(8,128)(2,1)S(1)}, u32[]{:S(2)}, u32[]{:S(2)}) %collective-permute-start.3) | collective-permute-done | bytes 131104 | tf_op jit(solution)/shard_map/ppermute | solution.py:465
  33.0 1.4 collective-permute-done.1
  34.7 2.8 %collective-permute-start.4 = (bf16[2,128,512]{2,1,0:T(8,128)(2,1)S(1)}, bf16[2,128,512]{2,1,0:T(8,128)(2,1)S(1)}, u32[]{:S(2)}, u32[]{:S(2)}) collective-permute-start(bf16[2,128,512]{2,1,0:T(8,128)(2,1)S(1)} %pad_maximum_fusion.1), channel_id=1, source_target_pairs={{0,6},{1,7},{2,0},{3,1},{4,2},{5,3},{6,4},{7,5},{8,14},{9,15},{10,... | collective-permute-start | bytes 786440 | tf_op jit(solution)/shard_map/ppermute | solution.py:465
  37.6 1.6 load_state.2.refs_7_.state_ref
  39.3 3.7 %collective-permute-done.2.refs_2_ = bf16[2,128,512]{2,1,0:T(8,128)(2,1)S(1)} collective-permute-done((bf16[2,128,512]{2,1,0:T(8,128)(2,1)S(1)}, bf16[2,128,512]{2,1,0:T(8,128)(2,1)S(1)}, u32[]{:S(2)}, u32[]{:S(2)}) %collective-permute-start.2) | collective-permute-done | bytes 262176 | tf_op jit(solution)/shard_map/ppermute | solution.py:465
  43.0 1.3 recur.2
  44.4 3.7 %collective-permute-start.6 = (bf16[128,256]{1,0:T(8,128)(2,1)S(1)}, bf16[128,256]{1,0:T(8,128)(2,1)S(1)}, u32[]{:S(2)}, u32[]{:S(2)}) collective-permute-start(bf16[128,256]{1,0:T(8,128)(2,1)S(1)} %get-tuple-element.36), channel_id=1, source_target_pairs={{0,4},{1,5},{2,6},{3,7},{4,0},{5,1},{6,2},{7,3},{8,12},{9,13},{10,... | collective-permute-start | bytes 196616 | tf_op jit(solution)/shard_map/ppermute | solution.py:465
  48.7 1.8 collective-permute-done.6
  50.5 1.0 collective-permute-done.5
  51.5 5.2 %all_gather.6.refs_0_ = bf16[8,128,256]{2,1,0:T(8,128)(2,1)S(1)} all-gather(bf16[4,128,256]{2,1,0:T(8,128)(2,1)S(1)} %pad_maximum_fusion.2), channel_id=1, replica_groups={{0,1},{2,3},{4,5},{6,7},{8,9},{10,11},{12,13},{14,15},{16,17},{18,19},{..., dimensions={0}, use_global_device_ids=true | all-gather | bytes 786432 | tf_op jit(solution)/shard_map/all_gather | solution.py:504
  56.7 1.6 close.2
  58.7 5.8 %collective-permute-start.10 = (bf16[128,512]{1,0:T(8,128)(2,1)S(1)}, bf16[128,512]{1,0:T(8,128)(2,1)S(1)}, u32[]{:S(2)}, u32[]{:S(2)}) collective-permute-start(bf16[128,512]{1,0:T(8,128)(2,1)S(1)} %get-tuple-element.40), channel_id=1, source_target_pairs={{0,120},{8,0},{16,8},{24,16},{32,24},{40,32},{48,40},{56,48},{64,5... | collective-permute-start | bytes 393224 | tf_op jit(solution)/shard_map/ppermute | solution.py:475
  64.5 2.7 %collective-permute-done.8 = bf16[128,512]{1,0:T(8,128)(2,1)S(1)} collective-permute-done((bf16[128,512]{1,0:T(8,128)(2,1)S(1)}, bf16[128,512]{1,0:T(8,128)(2,1)S(1)}, u32[]{:S(2)}, u32[]{:S(2)}) %collective-permute-start.8) | collective-permute-done | bytes 131104 | tf_op jit(solution)/shard_map/ppermute | solution.py:475
  67.2 6.1 %collective-permute-done.9 = bf16[128,512]{1,0:T(8,128)(2,1)S(1)} collective-permute-done((bf16[128,512]{1,0:T(8,128)(2,1)S(1)}, bf16[128,512]{1,0:T(8,128)(2,1)S(1)}, u32[]{:S(2)}, u32[]{:S(2)}) %collective-permute-start.9) | collective-permute-done | bytes 131104 | tf_op jit(solution)/shard_map/ppermute | solution.py:475
  73.5 2.6 %collective-permute-start.13 = (bf16[128,256]{1,0:T(8,128)(2,1)S(1)}, bf16[128,256]{1,0:T(8,128)(2,1)S(1)}, u32[]{:S(2)}, u32[]{:S(2)}) collective-permute-start(bf16[128,256]{1,0:T(8,128)(2,1)S(1)} %get-tuple-element.91), channel_id=1, source_target_pairs={{0,96},{8,104},{16,112},{24,120},{32,64},{40,72},{48,80},{56,88},{... | collective-permute-start | bytes 196616 | tf_op jit(solution)/shard_map/ppermute | solution.py:480
  76.1 0.9 own_rows.1
  77.1 2.6 %update_state.2.refs_0_ = f32[2,16,128,256]{3,2,1,0:T(8,128)} custom-call(bf16[128,128]{1,0:T(8,128)(2,1)S(1)} %get-tuple-element.42.wk_ref, bf16[128,256]{1,0:T(8,128)(2,1)S(1)} %get-tuple-element.43.v_ref, f32[16,1,128]{2,1,0:T(1,128)S(1)} %get-tuple-element.44.end_ref, f32[16,128,256]{2,1,0:T(8,128)S(1)} %load_state.2.refs_7_.state_ref), custom_call_target="tpu_custom_call" | custom-call | tf_op jit(solution)/shard_map/update_state/pallas_call | solution.py:371
  79.8 0.8 collective-permute-done.11
  80.6 0.4 collective-permute-done.13
  81.1 3.5 %collective-permute-start.12 = (bf16[128,256]{1,0:T(8,128)(2,1)S(1)}, bf16[128,256]{1,0:T(8,128)(2,1)S(1)}, u32[]{:S(2)}, u32[]{:S(2)}) collective-permute-start(bf16[128,256]{1,0:T(8,128)(2,1)S(1)} %get-tuple-element.88), channel_id=1, source_target_pairs={{0,96},{8,104},{16,112},{24,120},{32,64},{40,72},{48,80},{56,88},{... | collective-permute-start | bytes 196616 | tf_op jit(solution)/shard_map/ppermute | solution.py:480
  84.5 5.0 %collective-permute-start.14 = (bf16[128,256]{1,0:T(8,128)(2,1)S(1)}, bf16[128,256]{1,0:T(8,128)(2,1)S(1)}, u32[]{:S(2)}, u32[]{:S(2)}) collective-permute-start(bf16[128,256]{1,0:T(8,128)(2,1)S(1)} %get-tuple-element.89), channel_id=1, source_target_pairs={{0,32},{8,40},{16,48},{24,56},{32,0},{40,8},{48,16},{56,24},{64,96... | collective-permute-start | bytes 196616 | tf_op jit(solution)/shard_map/ppermute | solution.py:480
  89.5 2.1 %collective-permute-done.14 = bf16[128,256]{1,0:T(8,128)(2,1)S(1)} collective-permute-done((bf16[128,256]{1,0:T(8,128)(2,1)S(1)}, bf16[128,256]{1,0:T(8,128)(2,1)S(1)}, u32[]{:S(2)}, u32[]{:S(2)}) %collective-permute-start.14) | collective-permute-done | bytes 65568 | tf_op jit(solution)/shard_map/ppermute | solution.py:480
  91.7 5.2 %collective-permute-start.17 = (bf16[128,512]{1,0:T(8,128)(2,1)S(1)}, bf16[128,512]{1,0:T(8,128)(2,1)S(1)}, u32[]{:S(2)}, u32[]{:S(2)}) collective-permute-start(bf16[128,512]{1,0:T(8,128)(2,1)S(1)} %fusion.refs_0_), channel_id=1, source_target_pairs={{0,112},{8,120},{16,0},{24,8},{32,16},{40,24},{48,32},{56,40},{64,... | collective-permute-start | bytes 393224 | tf_op jit(solution)/shard_map/ppermute | solution.py:475
  96.9 2.5 %collective-permute-start.16 = (bf16[128,512]{1,0:T(8,128)(2,1)S(1)}, bf16[128,512]{1,0:T(8,128)(2,1)S(1)}, u32[]{:S(2)}, u32[]{:S(2)}) collective-permute-start(bf16[128,512]{1,0:T(8,128)(2,1)S(1)} %fusion.refs_0_), channel_id=1, source_target_pairs={{0,8},{8,16},{16,24},{24,32},{32,40},{40,48},{48,56},{56,64},{64,7... | collective-permute-start | bytes 393224 | tf_op jit(solution)/shard_map/ppermute | solution.py:475
  99.6 1.1 collective-permute-done.17.refs_3_
  100.7 1.3 collective-permute-done.16.refs_2_
  102.0 5.0 %collective-permute-done.15.refs_1_ = bf16[128,512]{1,0:T(8,128)(2,1)S(1)} collective-permute-done((bf16[128,512]{1,0:T(8,128)(2,1)S(1)}, bf16[128,512]{1,0:T(8,128)(2,1)S(1)}, u32[]{:S(2)}, u32[]{:S(2)}) %collective-permute-start.15) | collective-permute-done | bytes 131104 | tf_op jit(solution)/shard_map/ppermute | solution.py:475
  107.0 2.7 %project_next.3 = bf16[4,2,128,512]{3,2,1,0:T(8,128)(2,1)S(1)} custom-call(s32[32]{0:T(128)S(1)} %get-tuple-element.92.meta, f32[8,128]{1,0:T(8,128)S(1)} %plan.1.where_ref, bf16[128,512]{1,0:T(8,128)(2,1)S(1)} %fusion.refs_0_, bf16[128,512]{1,0:T(8,128)(2,1)S(1)} %collective-permute-done.15.refs_1_, bf16[128,512]{1,0:T(8,128)(2,1)S(1)} %collective-permute-done.16.refs_2_, ...), custom_call_target="tpu_custom_call" | custom-call | tf_op jit(solution)/shard_map/project_next/pallas_call | solution.py:160
  109.7 1.6 collective-permute-start.18
  111.3 2.7 %project_next.2.refs_0_ = bf16[4,2,128,512]{3,2,1,0:T(8,128)(2,1)S(1)} custom-call(s32[32]{0:T(128)S(1)} %get-tuple-element.70.meta, f32[8,128]{1,0:T(8,128)S(1)} %plan.1.where_ref, bf16[128,512]{1,0:T(8,128)(2,1)S(1)} %fusion.refs_0_, bf16[128,512]{1,0:T(8,128)(2,1)S(1)} %collective-permute-done.15.refs_1_, ...), custom_call_target="tpu_custom_call" | custom-call | tf_op jit(solution)/shard_map/project_next/pallas_call | solution.py:160
  114.2 1.0 collective-permute-start.21
  115.2 0.6 collective-permute-start.19
  115.8 3.6 %collective-permute-done.21 = bf16[128,512]{1,0:T(8,128)(2,1)S(1)} collective-permute-done((bf16[128,512]{1,0:T(8,128)(2,1)S(1)}, bf16[128,512]{1,0:T(8,128)(2,1)S(1)}, u32[]{:S(2)}, u32[]{:S(2)}) %collective-permute-start.21) | collective-permute-done | bytes 131104 | tf_op jit(solution)/shard_map/ppermute | solution.py:465
  119.3 1.8 collective-permute-done.19
  121.5 2.8 %collective-permute-start.22 = (bf16[2,128,512]{2,1,0:T(8,128)(2,1)S(1)}, bf16[2,128,512]{2,1,0:T(8,128)(2,1)S(1)}, u32[]{:S(2)}, u32[]{:S(2)}) collective-permute-start(bf16[2,128,512]{2,1,0:T(8,128)(2,1)S(1)} %pad_maximum_fusion.4), channel_id=1, source_target_pairs={{0,6},{1,7},{2,0},{3,1},{4,2},{5,3},{6,4},{7,5},{8,14},{9,15},{10,... | collective-permute-start | bytes 786440 | tf_op jit(solution)/shard_map/ppermute | solution.py:465
  124.2 1.6 load_state.3.refs_7_.state_ref
  125.8 3.5 %collective-permute-done.20.refs_2_ = bf16[2,128,512]{2,1,0:T(8,128)(2,1)S(1)} collective-permute-done((bf16[2,128,512]{2,1,0:T(8,128)(2,1)S(1)}, bf16[2,128,512]{2,1,0:T(8,128)(2,1)S(1)}, u32[]{:S(2)}, u32[]{:S(2)}) %collective-permute-start.20) | collective-permute-done | bytes 262176 | tf_op jit(solution)/shard_map/ppermute | solution.py:465
  129.3 1.8 recur.3
  131.1 3.7 %collective-permute-start.24 = (bf16[128,256]{1,0:T(8,128)(2,1)S(1)}, bf16[128,256]{1,0:T(8,128)(2,1)S(1)}, u32[]{:S(2)}, u32[]{:S(2)}) collective-permute-start(bf16[128,256]{1,0:T(8,128)(2,1)S(1)} %get-tuple-element.50), channel_id=1, source_target_pairs={{0,4},{1,5},{2,6},{3,7},{4,0},{5,1},{6,2},{7,3},{8,12},{9,13},{10,... | collective-permute-start | bytes 196616 | tf_op jit(solution)/shard_map/ppermute | solution.py:465
  134.8 0.6 collective-permute-done.25
  135.4 1.7 collective-permute-done.24
  137.1 1.0 collective-permute-done.23
  138.2 5.6 %all_gather.7.refs_0_ = bf16[8,128,256]{2,1,0:T(8,128)(2,1)S(1)} all-gather(bf16[4,128,256]{2,1,0:T(8,128)(2,1)S(1)} %pad_maximum_fusion.5), channel_id=1, replica_groups={{0,1},{2,3},{4,5},{6,7},{8,9},{10,11},{12,13},{14,15},{16,17},{18,19},{..., dimensions={0}, use_global_device_ids=true | all-gather | bytes 786432 | tf_op jit(solution)/shard_map/all_gather | solution.py:504
  143.8 1.6 close.3
  145.5 1.3 collective-permute-start.26
  146.8 2.4 %collective-permute-start.27 = (bf16[128,512]{1,0:T(8,128)(2,1)S(1)}, bf16[128,512]{1,0:T(8,128)(2,1)S(1)}, u32[]{:S(2)}, u32[]{:S(2)}) collective-permute-start(bf16[128,512]{1,0:T(8,128)(2,1)S(1)} %get-tuple-element.53), channel_id=1, source_target_pairs={{0,8},{8,16},{16,24},{24,32},{32,40},{40,48},{48,56},{56,64},{64,7... | collective-permute-start | bytes 393224 | tf_op jit(solution)/shard_map/ppermute | solution.py:475
  149.5 4.2 %collective-permute-done.26 = bf16[128,512]{1,0:T(8,128)(2,1)S(1)} collective-permute-done((bf16[128,512]{1,0:T(8,128)(2,1)S(1)}, bf16[128,512]{1,0:T(8,128)(2,1)S(1)}, u32[]{:S(2)}, u32[]{:S(2)}) %collective-permute-start.26) | collective-permute-done | bytes 131104 | tf_op jit(solution)/shard_map/ppermute | solution.py:475
  153.7 2.5 %collective-permute-done.27 = bf16[128,512]{1,0:T(8,128)(2,1)S(1)} collective-permute-done((bf16[128,512]{1,0:T(8,128)(2,1)S(1)}, bf16[128,512]{1,0:T(8,128)(2,1)S(1)}, u32[]{:S(2)}, u32[]{:S(2)}) %collective-permute-start.27) | collective-permute-done | bytes 131104 | tf_op jit(solution)/shard_map/ppermute | solution.py:475
  156.3 4.6 %collective-permute-start.29 = (bf16[128,256]{1,0:T(8,128)(2,1)S(1)}, bf16[128,256]{1,0:T(8,128)(2,1)S(1)}, u32[]{:S(2)}, u32[]{:S(2)}) collective-permute-start(bf16[128,256]{1,0:T(8,128)(2,1)S(1)} %get-tuple-element.86), channel_id=1, source_target_pairs={{0,32},{8,40},{16,48},{24,56},{32,0},{40,8},{48,16},{56,24},{64,96... | collective-permute-start | bytes 196616 | tf_op jit(solution)/shard_map/ppermute | solution.py:480
  160.9 4.2 %collective-permute-start.31 = (bf16[128,256]{1,0:T(8,128)(2,1)S(1)}, bf16[128,256]{1,0:T(8,128)(2,1)S(1)}, u32[]{:S(2)}, u32[]{:S(2)}) collective-permute-start(bf16[128,256]{1,0:T(8,128)(2,1)S(1)} %get-tuple-element.87), channel_id=1, source_target_pairs={{0,96},{8,104},{16,112},{24,120},{32,64},{40,72},{48,80},{56,88},{... | collective-permute-start | bytes 196616 | tf_op jit(solution)/shard_map/ppermute | solution.py:480
  165.1 2.6 %update_state.3 = f32[2,16,128,256]{3,2,1,0:T(8,128)} custom-call(bf16[128,128]{1,0:T(8,128)(2,1)S(1)} %get-tuple-element.56.wk_ref, bf16[128,256]{1,0:T(8,128)(2,1)S(1)} %get-tuple-element.57.v_ref, f32[16,1,128]{2,1,0:T(1,128)S(1)} %get-tuple-element.58.end_ref, f32[16,128,256]{2,1,0:T(8,128)S(1)} %load_state.3.refs_7_.state_ref, ...), custom_call_target="tpu_custom_call", output_to_operand_aliasing={{}: (4, {})} | custom-call | tf_op jit(solution)/shard_map/update_state/pallas_call | solution.py:371
  167.7 1.8 collective-permute-done.31
  169.5 6.4 %collective-permute-start.30 = (bf16[128,256]{1,0:T(8,128)(2,1)S(1)}, bf16[128,256]{1,0:T(8,128)(2,1)S(1)}, u32[]{:S(2)}, u32[]{:S(2)}) collective-permute-start(bf16[128,256]{1,0:T(8,128)(2,1)S(1)} %get-tuple-element.84), channel_id=1, source_target_pairs={{0,96},{8,104},{16,112},{24,120},{32,64},{40,72},{48,80},{56,88},{... | collective-permute-start | bytes 196616 | tf_op jit(solution)/shard_map/ppermute | solution.py:480
  175.9 4.4 %collective-permute-done.30 = bf16[128,256]{1,0:T(8,128)(2,1)S(1)} collective-permute-done((bf16[128,256]{1,0:T(8,128)(2,1)S(1)}, bf16[128,256]{1,0:T(8,128)(2,1)S(1)}, u32[]{:S(2)}, u32[]{:S(2)}) %collective-permute-start.30) | collective-permute-done | bytes 65568 | tf_op jit(solution)/shard_map/ppermute | solution.py:480
  180.4 6.9 %collective-permute-done.32 = bf16[128,256]{1,0:T(8,128)(2,1)S(1)} collective-permute-done((bf16[128,256]{1,0:T(8,128)(2,1)S(1)}, bf16[128,256]{1,0:T(8,128)(2,1)S(1)}, u32[]{:S(2)}, u32[]{:S(2)}) %collective-permute-start.32) | collective-permute-done | bytes 65568 | tf_op jit(solution)/shard_map/ppermute | solution.py:480
  187.3 0.9 collective-permute-start.35
  188.2 2.5 %collective-permute-start.34 = (bf16[128,512]{1,0:T(8,128)(2,1)S(1)}, bf16[128,512]{1,0:T(8,128)(2,1)S(1)}, u32[]{:S(2)}, u32[]{:S(2)}) collective-permute-start(bf16[128,512]{1,0:T(8,128)(2,1)S(1)} %fusion.1.refs_0_), channel_id=1, source_target_pairs={{0,8},{8,16},{16,24},{24,32},{32,40},{40,48},{48,56},{56,64},{64,7... | collective-permute-start | bytes 393224 | tf_op jit(solution)/shard_map/ppermute | solution.py:475
  190.9 4.6 %collective-permute-done.35.refs_3_ = bf16[128,512]{1,0:T(8,128)(2,1)S(1)} collective-permute-done((bf16[128,512]{1,0:T(8,128)(2,1)S(1)}, bf16[128,512]{1,0:T(8,128)(2,1)S(1)}, u32[]{:S(2)}, u32[]{:S(2)}) %collective-permute-start.35) | collective-permute-done | bytes 131104 | tf_op jit(solution)/shard_map/ppermute | solution.py:475
  195.5 4.3 %collective-permute-done.33.refs_1_ = bf16[128,512]{1,0:T(8,128)(2,1)S(1)} collective-permute-done((bf16[128,512]{1,0:T(8,128)(2,1)S(1)}, bf16[128,512]{1,0:T(8,128)(2,1)S(1)}, u32[]{:S(2)}, u32[]{:S(2)}) %collective-permute-start.33) | collective-permute-done | bytes 131104 | tf_op jit(solution)/shard_map/ppermute | solution.py:475
  199.8 3.3 %finish.1 = bf16[1024,512]{1,0:T(8,128)(2,1)} custom-call(s32[32]{0:T(128)S(1)} %get-tuple-element.71.meta, f32[8,128]{1,0:T(8,128)S(1)} %plan.1.where_ref, bf16[128,512]{1,0:T(8,128)(2,1)S(1)} %fusion.1.refs_0_, bf16[128,512]{1,0:T(8,128)(2,1)S(1)} %collective-permute-done.33.refs_1_, bf16[128,512]{1,0:T(8,128)(2,1)S(1)} %collective-permute-done.34.refs_2_, ...), custom_call_target="tpu_custom_call" | custom-call | tf_op jit(solution)/shard_map/finish/pallas_call | solution.py:182
  (77 shorter events, 3.5 us)
Async XLA Ops:
  3.8 23.8 %collective-permute-start = (bf16[4,2,128,512]{3,2,1,0:T(8,128)(2,1)S(1)}, bf16[4,2,128,512]{3,2,1,0:T(8,128)(2,1)S(1)}, u32[]{:S(2)}, u32[]{:S(2)}) collective-permute-start(bf16[4,2,128,512]{3,2,1,0:T(8,128)(2,1)S(1)} %project_first.3), channel_id=1, source_target_pairs={{0,1},{1,0},{2,3},{3,2},{4,5},{5,4},{6,7},{7,6},{8,9},{9,8},{10,11... | collective-permute-start | bytes 3145736 | tf_op jit(solution)/shard_map/ppermute | solution.py:470
  24.3 13.1 %copy-start.11 = (f32[16,8,1]{0,2,1:T(1,128)S(1)}, f32[16,8,1]{0,2,1:T(1,128)}, u32[]{:S(2)}) copy-start(f32[16,8,1]{0,2,1:T(1,128)} %param.22) | copy-start | bytes 1540
  27.7 5.2 %collective-permute-start.3 = (bf16[128,512]{1,0:T(8,128)(2,1)S(1)}, bf16[128,512]{1,0:T(8,128)(2,1)S(1)}, u32[]{:S(2)}, u32[]{:S(2)}) collective-permute-start(bf16[128,512]{1,0:T(8,128)(2,1)S(1)} %get-tuple-element.79), channel_id=1, source_target_pairs={{0,6},{1,7},{2,0},{3,1},{4,2},{5,3},{6,4},{7,5},{8,14},{9,15},{10,... | collective-permute-start | bytes 393224 | tf_op jit(solution)/shard_map/ppermute | solution.py:465
  27.9 15.1 %copy-start.8 = (s32[16]{0:T(128)S(1)}, s32[16]{0:T(128)}, u32[]{:S(2)}) copy-start(s32[16]{0:T(128)} %lens.7) | copy-start | bytes 196
  27.9 15.0 %copy-start.9 = (f32[2,128]{1,0:T(2,128)S(1)}, f32[2,128]{1,0:T(2,128)}, u32[]{:S(2)}) copy-start(f32[2,128]{1,0:T(2,128)} %refs_4_.7) | copy-start | bytes 3076
  27.9 15.0 %copy-start.10 = (bf16[2,256]{1,0:T(2,128)(2,1)S(1)}, bf16[2,256]{1,0:T(2,128)(2,1)}, u32[]{:S(2)}) copy-start(bf16[2,256]{1,0:T(2,128)(2,1)} %refs_6_.7) | copy-start | bytes 3076
  27.9 6.5 %collective-permute-start.1 = (bf16[128,512]{1,0:T(8,128)(2,1)S(1)}, bf16[128,512]{1,0:T(8,128)(2,1)S(1)}, u32[]{:S(2)}, u32[]{:S(2)}) collective-permute-start(bf16[128,512]{1,0:T(8,128)(2,1)S(1)} %get-tuple-element.81), channel_id=1, source_target_pairs={{0,2},{1,3},{2,4},{3,5},{4,6},{5,7},{6,0},{7,1},{8,10},{9,11},{10,... | collective-permute-start | bytes 393224 | tf_op jit(solution)/shard_map/ppermute | solution.py:465
  34.5 8.4 %collective-permute-start.2 = (bf16[2,128,512]{2,1,0:T(8,128)(2,1)S(1)}, bf16[2,128,512]{2,1,0:T(8,128)(2,1)S(1)}, u32[]{:S(2)}, u32[]{:S(2)}) collective-permute-start(bf16[2,128,512]{2,1,0:T(8,128)(2,1)S(1)} %pad_maximum_fusion), channel_id=1, source_target_pairs={{0,2},{1,3},{2,4},{3,5},{4,6},{5,7},{6,0},{7,1},{8,10},{9,11},{10,... | collective-permute-start | bytes 786440 | tf_op jit(solution)/shard_map/ppermute | solution.py:465
  34.7 8.2 %collective-permute-start.4 = (bf16[2,128,512]{2,1,0:T(8,128)(2,1)S(1)}, bf16[2,128,512]{2,1,0:T(8,128)(2,1)S(1)}, u32[]{:S(2)}, u32[]{:S(2)}) collective-permute-start(bf16[2,128,512]{2,1,0:T(8,128)(2,1)S(1)} %pad_maximum_fusion.1), channel_id=1, source_target_pairs={{0,6},{1,7},{2,0},{3,1},{4,2},{5,3},{6,4},{7,5},{8,14},{9,15},{10,... | collective-permute-start | bytes 786440 | tf_op jit(solution)/shard_map/ppermute | solution.py:465
  39.2 17.5 %copy-start.6 = (bf16[2,256,512]{2,1,0:T(8,128)(2,1)S(1)}, bf16[2,256,512]{2,1,0:T(8,128)(2,1)}, u32[]{:S(2)}) copy-start(bf16[2,256,512]{2,1,0:T(8,128)(2,1)} %refs_1_.3) | copy-start | bytes 1572868
  39.2 36.8 %copy-start = (bf16[128,8,512]{2,1,0:T(8,128)(2,1)S(1)}, bf16[128,8,512]{2,1,0:T(8,128)(2,1)}, u32[]{:S(2)}) copy-start(bf16[128,8,512]{2,1,0:T(8,128)(2,1)} %param.13) | copy-start | bytes 3145732
  44.2 4.4 %collective-permute-start.7 = (bf16[128,256]{1,0:T(8,128)(2,1)S(1)}, bf16[128,256]{1,0:T(8,128)(2,1)S(1)}, u32[]{:S(2)}, u32[]{:S(2)}) collective-permute-start(bf16[128,256]{1,0:T(8,128)(2,1)S(1)} %get-tuple-element.36), channel_id=1, source_target_pairs={{0,2},{1,3},{2,4},{3,5},{4,6},{5,7},{6,0},{7,1},{8,10},{9,11},{10,... | collective-permute-start | bytes 196616 | tf_op jit(solution)/shard_map/ppermute | solution.py:465
  44.4 6.1 %collective-permute-start.6 = (bf16[128,256]{1,0:T(8,128)(2,1)S(1)}, bf16[128,256]{1,0:T(8,128)(2,1)S(1)}, u32[]{:S(2)}, u32[]{:S(2)}) collective-permute-start(bf16[128,256]{1,0:T(8,128)(2,1)S(1)} %get-tuple-element.36), channel_id=1, source_target_pairs={{0,4},{1,5},{2,6},{3,7},{4,0},{5,1},{6,2},{7,3},{8,12},{9,13},{10,... | collective-permute-start | bytes 196616 | tf_op jit(solution)/shard_map/ppermute | solution.py:465
  48.1 3.4 %collective-permute-start.5 = (bf16[128,256]{1,0:T(8,128)(2,1)S(1)}, bf16[128,256]{1,0:T(8,128)(2,1)S(1)}, u32[]{:S(2)}, u32[]{:S(2)}) collective-permute-start(bf16[128,256]{1,0:T(8,128)(2,1)S(1)} %get-tuple-element.36), channel_id=1, source_target_pairs={{0,6},{1,7},{2,0},{3,1},{4,2},{5,3},{6,4},{7,5},{8,14},{9,15},{10,... | collective-permute-start | bytes 196616 | tf_op jit(solution)/shard_map/ppermute | solution.py:465
  58.4 8.8 %collective-permute-start.8 = (bf16[128,512]{1,0:T(8,128)(2,1)S(1)}, bf16[128,512]{1,0:T(8,128)(2,1)S(1)}, u32[]{:S(2)}, u32[]{:S(2)}) collective-permute-start(bf16[128,512]{1,0:T(8,128)(2,1)S(1)} %get-tuple-element.38), channel_id=1, source_target_pairs={{0,16},{8,24},{16,32},{24,40},{32,48},{40,56},{48,64},{56,72},{64,... | collective-permute-start | bytes 393224 | tf_op jit(solution)/shard_map/ppermute | solution.py:475
  58.5 14.7 %collective-permute-start.9 = (bf16[128,512]{1,0:T(8,128)(2,1)S(1)}, bf16[128,512]{1,0:T(8,128)(2,1)S(1)}, u32[]{:S(2)}, u32[]{:S(2)}) collective-permute-start(bf16[128,512]{1,0:T(8,128)(2,1)S(1)} %get-tuple-element.39), channel_id=1, source_target_pairs={{0,8},{8,16},{16,24},{24,32},{32,40},{40,48},{48,56},{56,64},{64,7... | collective-permute-start | bytes 393224 | tf_op jit(solution)/shard_map/ppermute | solution.py:475
  58.7 14.6 %collective-permute-start.10 = (bf16[128,512]{1,0:T(8,128)(2,1)S(1)}, bf16[128,512]{1,0:T(8,128)(2,1)S(1)}, u32[]{:S(2)}, u32[]{:S(2)}) collective-permute-start(bf16[128,512]{1,0:T(8,128)(2,1)S(1)} %get-tuple-element.40), channel_id=1, source_target_pairs={{0,120},{8,0},{16,8},{24,16},{32,24},{40,32},{48,40},{56,48},{64,5... | collective-permute-start | bytes 393224 | tf_op jit(solution)/shard_map/ppermute | solution.py:475
  73.4 7.2 %collective-permute-start.11 = (bf16[128,256]{1,0:T(8,128)(2,1)S(1)}, bf16[128,256]{1,0:T(8,128)(2,1)S(1)}, u32[]{:S(2)}, u32[]{:S(2)}) collective-permute-start(bf16[128,256]{1,0:T(8,128)(2,1)S(1)} %get-tuple-element.90), channel_id=1, source_target_pairs={{0,32},{8,40},{16,48},{24,56},{32,0},{40,8},{48,16},{56,24},{64,96... | collective-permute-start | bytes 196616 | tf_op jit(solution)/shard_map/ppermute | solution.py:480
  73.5 7.5 %collective-permute-start.13 = (bf16[128,256]{1,0:T(8,128)(2,1)S(1)}, bf16[128,256]{1,0:T(8,128)(2,1)S(1)}, u32[]{:S(2)}, u32[]{:S(2)}) collective-permute-start(bf16[128,256]{1,0:T(8,128)(2,1)S(1)} %get-tuple-element.91), channel_id=1, source_target_pairs={{0,96},{8,104},{16,112},{24,120},{32,64},{40,72},{48,80},{56,88},{... | collective-permute-start | bytes 196616 | tf_op jit(solution)/shard_map/ppermute | solution.py:480
  77.0 29.9 %copy-start.1 = (bf16[2,512,256]{2,1,0:T(8,128)(2,1)S(1)}, bf16[2,512,256]{2,1,0:T(8,128)(2,1)}, u32[]{:S(2)}) copy-start(bf16[2,512,256]{2,1,0:T(8,128)(2,1)} %refs_7_.3) | copy-start | bytes 1572868
  77.1 29.9 %copy-start.2 = (bf16[2,512,256]{2,1,0:T(8,128)(2,1)S(1)}, bf16[2,512,256]{2,1,0:T(8,128)(2,1)}, u32[]{:S(2)}) copy-start(bf16[2,512,256]{2,1,0:T(8,128)(2,1)} %refs_8_.3) | copy-start | bytes 1572868
  77.1 29.9 %copy-start.3 = (bf16[2,512,128]{2,1,0:T(8,128)(2,1)S(1)}, bf16[2,512,128]{2,1,0:T(8,128)(2,1)}, u32[]{:S(2)}) copy-start(bf16[2,512,128]{2,1,0:T(8,128)(2,1)} %refs_5_.3) | copy-start | bytes 786436
  77.1 29.9 %copy-start.4 = (bf16[2,512,128]{2,1,0:T(8,128)(2,1)S(1)}, bf16[2,512,128]{2,1,0:T(8,128)(2,1)}, u32[]{:S(2)}) copy-start(bf16[2,512,128]{2,1,0:T(8,128)(2,1)} %refs_6_.6) | copy-start | bytes 786436
  77.1 29.8 %copy-start.5 = (bf16[2,512,128]{2,1,0:T(8,128)(2,1)S(1)}, bf16[2,512,128]{2,1,0:T(8,128)(2,1)}, u32[]{:S(2)}) copy-start(bf16[2,512,128]{2,1,0:T(8,128)(2,1)} %refs_9_.3) | copy-start | bytes 786436
  77.1 29.8 %copy-start.7 = (bf16[2,512]{1,0:T(2,128)(2,1)S(1)}, bf16[2,512]{1,0:T(2,128)(2,1)}, u32[]{:S(2)}) copy-start(bf16[2,512]{1,0:T(2,128)(2,1)} %refs_4_.6) | copy-start | bytes 6148
  81.1 8.4 %collective-permute-start.12 = (bf16[128,256]{1,0:T(8,128)(2,1)S(1)}, bf16[128,256]{1,0:T(8,128)(2,1)S(1)}, u32[]{:S(2)}, u32[]{:S(2)}) collective-permute-start(bf16[128,256]{1,0:T(8,128)(2,1)S(1)} %get-tuple-element.88), channel_id=1, source_target_pairs={{0,96},{8,104},{16,112},{24,120},{32,64},{40,72},{48,80},{56,88},{... | collective-permute-start | bytes 196616 | tf_op jit(solution)/shard_map/ppermute | solution.py:480
  84.5 7.1 %collective-permute-start.14 = (bf16[128,256]{1,0:T(8,128)(2,1)S(1)}, bf16[128,256]{1,0:T(8,128)(2,1)S(1)}, u32[]{:S(2)}, u32[]{:S(2)}) collective-permute-start(bf16[128,256]{1,0:T(8,128)(2,1)S(1)} %get-tuple-element.89), channel_id=1, source_target_pairs={{0,32},{8,40},{16,48},{24,56},{32,0},{40,8},{48,16},{56,24},{64,96... | collective-permute-start | bytes 196616 | tf_op jit(solution)/shard_map/ppermute | solution.py:480
  91.7 9.0 %collective-permute-start.17 = (bf16[128,512]{1,0:T(8,128)(2,1)S(1)}, bf16[128,512]{1,0:T(8,128)(2,1)S(1)}, u32[]{:S(2)}, u32[]{:S(2)}) collective-permute-start(bf16[128,512]{1,0:T(8,128)(2,1)S(1)} %fusion.refs_0_), channel_id=1, source_target_pairs={{0,112},{8,120},{16,0},{24,8},{32,16},{40,24},{48,32},{56,40},{64,... | collective-permute-start | bytes 393224 | tf_op jit(solution)/shard_map/ppermute | solution.py:475
  96.9 5.0 %collective-permute-start.16 = (bf16[128,512]{1,0:T(8,128)(2,1)S(1)}, bf16[128,512]{1,0:T(8,128)(2,1)S(1)}, u32[]{:S(2)}, u32[]{:S(2)}) collective-permute-start(bf16[128,512]{1,0:T(8,128)(2,1)S(1)} %fusion.refs_0_), channel_id=1, source_target_pairs={{0,8},{8,16},{16,24},{24,32},{32,40},{40,48},{48,56},{56,64},{64,7... | collective-permute-start | bytes 393224 | tf_op jit(solution)/shard_map/ppermute | solution.py:475
  99.4 7.5 %collective-permute-start.15 = (bf16[128,512]{1,0:T(8,128)(2,1)S(1)}, bf16[128,512]{1,0:T(8,128)(2,1)S(1)}, u32[]{:S(2)}, u32[]{:S(2)}) collective-permute-start(bf16[128,512]{1,0:T(8,128)(2,1)S(1)} %fusion.refs_0_), channel_id=1, source_target_pairs={{0,120},{8,0},{16,8},{24,16},{32,24},{40,32},{48,40},{56,48},{64,5... | collective-permute-start | bytes 393224 | tf_op jit(solution)/shard_map/ppermute | solution.py:475
  109.7 4.3 %collective-permute-start.18 = (bf16[4,2,128,512]{3,2,1,0:T(8,128)(2,1)S(1)}, bf16[4,2,128,512]{3,2,1,0:T(8,128)(2,1)S(1)}, u32[]{:S(2)}, u32[]{:S(2)}) collective-permute-start(bf16[4,2,128,512]{3,2,1,0:T(8,128)(2,1)S(1)} %project_next.3), channel_id=1, source_target_pairs={{0,1},{1,0},{2,3},{3,2},{4,5},{5,4},{6,7},{7,6},{8,9},{9,8},{10,11... | collective-permute-start | bytes 3145736 | tf_op jit(solution)/shard_map/ppermute | solution.py:470
  114.2 5.1 %collective-permute-start.21 = (bf16[128,512]{1,0:T(8,128)(2,1)S(1)}, bf16[128,512]{1,0:T(8,128)(2,1)S(1)}, u32[]{:S(2)}, u32[]{:S(2)}) collective-permute-start(bf16[128,512]{1,0:T(8,128)(2,1)S(1)} %get-tuple-element.73), channel_id=1, source_target_pairs={{0,6},{1,7},{2,0},{3,1},{4,2},{5,3},{6,4},{7,5},{8,14},{9,15},{10,... | collective-permute-start | bytes 393224 | tf_op jit(solution)/shard_map/ppermute | solution.py:465
  115.2 5.9 %collective-permute-start.19 = (bf16[128,512]{1,0:T(8,128)(2,1)S(1)}, bf16[128,512]{1,0:T(8,128)(2,1)S(1)}, u32[]{:S(2)}, u32[]{:S(2)}) collective-permute-start(bf16[128,512]{1,0:T(8,128)(2,1)S(1)} %get-tuple-element.75), channel_id=1, source_target_pairs={{0,2},{1,3},{2,4},{3,5},{4,6},{5,7},{6,0},{7,1},{8,10},{9,11},{10,... | collective-permute-start | bytes 393224 | tf_op jit(solution)/shard_map/ppermute | solution.py:465
  121.3 8.0 %collective-permute-start.20 = (bf16[2,128,512]{2,1,0:T(8,128)(2,1)S(1)}, bf16[2,128,512]{2,1,0:T(8,128)(2,1)S(1)}, u32[]{:S(2)}, u32[]{:S(2)}) collective-permute-start(bf16[2,128,512]{2,1,0:T(8,128)(2,1)S(1)} %pad_maximum_fusion.3), channel_id=1, source_target_pairs={{0,2},{1,3},{2,4},{3,5},{4,6},{5,7},{6,0},{7,1},{8,10},{9,11},{10,... | collective-permute-start | bytes 786440 | tf_op jit(solution)/shard_map/ppermute | solution.py:465
  121.5 7.8 %collective-permute-start.22 = (bf16[2,128,512]{2,1,0:T(8,128)(2,1)S(1)}, bf16[2,128,512]{2,1,0:T(8,128)(2,1)S(1)}, u32[]{:S(2)}, u32[]{:S(2)}) collective-permute-start(bf16[2,128,512]{2,1,0:T(8,128)(2,1)S(1)} %pad_maximum_fusion.4), channel_id=1, source_target_pairs={{0,6},{1,7},{2,0},{3,1},{4,2},{5,3},{6,4},{7,5},{8,14},{9,15},{10,... | collective-permute-start | bytes 786440 | tf_op jit(solution)/shard_map/ppermute | solution.py:465
  131.1 4.3 %collective-permute-start.25 = (bf16[128,256]{1,0:T(8,128)(2,1)S(1)}, bf16[128,256]{1,0:T(8,128)(2,1)S(1)}, u32[]{:S(2)}, u32[]{:S(2)}) collective-permute-start(bf16[128,256]{1,0:T(8,128)(2,1)S(1)} %get-tuple-element.50), channel_id=1, source_target_pairs={{0,2},{1,3},{2,4},{3,5},{4,6},{5,7},{6,0},{7,1},{8,10},{9,11},{10,... | collective-permute-start | bytes 196616 | tf_op jit(solution)/shard_map/ppermute | solution.py:465
  131.1 6.1 %collective-permute-start.24 = (bf16[128,256]{1,0:T(8,128)(2,1)S(1)}, bf16[128,256]{1,0:T(8,128)(2,1)S(1)}, u32[]{:S(2)}, u32[]{:S(2)}) collective-permute-start(bf16[128,256]{1,0:T(8,128)(2,1)S(1)} %get-tuple-element.50), channel_id=1, source_target_pairs={{0,4},{1,5},{2,6},{3,7},{4,0},{5,1},{6,2},{7,3},{8,12},{9,13},{10,... | collective-permute-start | bytes 196616 | tf_op jit(solution)/shard_map/ppermute | solution.py:465
  134.8 3.4 %collective-permute-start.23 = (bf16[128,256]{1,0:T(8,128)(2,1)S(1)}, bf16[128,256]{1,0:T(8,128)(2,1)S(1)}, u32[]{:S(2)}, u32[]{:S(2)}) collective-permute-start(bf16[128,256]{1,0:T(8,128)(2,1)S(1)} %get-tuple-element.50), channel_id=1, source_target_pairs={{0,6},{1,7},{2,0},{3,1},{4,2},{5,3},{6,4},{7,5},{8,14},{9,15},{10,... | collective-permute-start | bytes 196616 | tf_op jit(solution)/shard_map/ppermute | solution.py:465
  145.5 8.2 %collective-permute-start.26 = (bf16[128,512]{1,0:T(8,128)(2,1)S(1)}, bf16[128,512]{1,0:T(8,128)(2,1)S(1)}, u32[]{:S(2)}, u32[]{:S(2)}) collective-permute-start(bf16[128,512]{1,0:T(8,128)(2,1)S(1)} %get-tuple-element.52), channel_id=1, source_target_pairs={{0,16},{8,24},{16,32},{24,40},{32,48},{40,56},{48,64},{56,72},{64,... | collective-permute-start | bytes 393224 | tf_op jit(solution)/shard_map/ppermute | solution.py:475
  146.8 9.4 %collective-permute-start.27 = (bf16[128,512]{1,0:T(8,128)(2,1)S(1)}, bf16[128,512]{1,0:T(8,128)(2,1)S(1)}, u32[]{:S(2)}, u32[]{:S(2)}) collective-permute-start(bf16[128,512]{1,0:T(8,128)(2,1)S(1)} %get-tuple-element.53), channel_id=1, source_target_pairs={{0,8},{8,16},{16,24},{24,32},{32,40},{40,48},{48,56},{56,64},{64,7... | collective-permute-start | bytes 393224 | tf_op jit(solution)/shard_map/ppermute | solution.py:475
  149.2 7.0 %collective-permute-start.28 = (bf16[128,512]{1,0:T(8,128)(2,1)S(1)}, bf16[128,512]{1,0:T(8,128)(2,1)S(1)}, u32[]{:S(2)}, u32[]{:S(2)}) collective-permute-start(bf16[128,512]{1,0:T(8,128)(2,1)S(1)} %get-tuple-element.54), channel_id=1, source_target_pairs={{0,120},{8,0},{16,8},{24,16},{32,24},{40,32},{48,40},{56,48},{64,5... | collective-permute-start | bytes 393224 | tf_op jit(solution)/shard_map/ppermute | solution.py:475
  156.3 11.4 %collective-permute-start.29 = (bf16[128,256]{1,0:T(8,128)(2,1)S(1)}, bf16[128,256]{1,0:T(8,128)(2,1)S(1)}, u32[]{:S(2)}, u32[]{:S(2)}) collective-permute-start(bf16[128,256]{1,0:T(8,128)(2,1)S(1)} %get-tuple-element.86), channel_id=1, source_target_pairs={{0,32},{8,40},{16,48},{24,56},{32,0},{40,8},{48,16},{56,24},{64,96... | collective-permute-start | bytes 196616 | tf_op jit(solution)/shard_map/ppermute | solution.py:480
  160.9 8.6 %collective-permute-start.31 = (bf16[128,256]{1,0:T(8,128)(2,1)S(1)}, bf16[128,256]{1,0:T(8,128)(2,1)S(1)}, u32[]{:S(2)}, u32[]{:S(2)}) collective-permute-start(bf16[128,256]{1,0:T(8,128)(2,1)S(1)} %get-tuple-element.87), channel_id=1, source_target_pairs={{0,96},{8,104},{16,112},{24,120},{32,64},{40,72},{48,80},{56,88},{... | collective-permute-start | bytes 196616 | tf_op jit(solution)/shard_map/ppermute | solution.py:480
  169.5 10.8 %collective-permute-start.30 = (bf16[128,256]{1,0:T(8,128)(2,1)S(1)}, bf16[128,256]{1,0:T(8,128)(2,1)S(1)}, u32[]{:S(2)}, u32[]{:S(2)}) collective-permute-start(bf16[128,256]{1,0:T(8,128)(2,1)S(1)} %get-tuple-element.84), channel_id=1, source_target_pairs={{0,96},{8,104},{16,112},{24,120},{32,64},{40,72},{48,80},{56,88},{... | collective-permute-start | bytes 196616 | tf_op jit(solution)/shard_map/ppermute | solution.py:480
  175.9 11.4 %collective-permute-start.32 = (bf16[128,256]{1,0:T(8,128)(2,1)S(1)}, bf16[128,256]{1,0:T(8,128)(2,1)S(1)}, u32[]{:S(2)}, u32[]{:S(2)}) collective-permute-start(bf16[128,256]{1,0:T(8,128)(2,1)S(1)} %get-tuple-element.85), channel_id=1, source_target_pairs={{0,32},{8,40},{16,48},{24,56},{32,0},{40,8},{48,16},{56,24},{64,96... | collective-permute-start | bytes 196616 | tf_op jit(solution)/shard_map/ppermute | solution.py:480
  187.3 8.1 %collective-permute-start.35 = (bf16[128,512]{1,0:T(8,128)(2,1)S(1)}, bf16[128,512]{1,0:T(8,128)(2,1)S(1)}, u32[]{:S(2)}, u32[]{:S(2)}) collective-permute-start(bf16[128,512]{1,0:T(8,128)(2,1)S(1)} %fusion.1.refs_0_), channel_id=1, source_target_pairs={{0,112},{8,120},{16,0},{24,8},{32,16},{40,24},{48,32},{56,40},{64,... | collective-permute-start | bytes 393224 | tf_op jit(solution)/shard_map/ppermute | solution.py:475
  188.2 7.2 %collective-permute-start.34 = (bf16[128,512]{1,0:T(8,128)(2,1)S(1)}, bf16[128,512]{1,0:T(8,128)(2,1)S(1)}, u32[]{:S(2)}, u32[]{:S(2)}) collective-permute-start(bf16[128,512]{1,0:T(8,128)(2,1)S(1)} %fusion.1.refs_0_), channel_id=1, source_target_pairs={{0,8},{8,16},{16,24},{24,32},{32,40},{40,48},{48,56},{56,64},{64,7... | collective-permute-start | bytes 393224 | tf_op jit(solution)/shard_map/ppermute | solution.py:475
  190.8 9.0 %collective-permute-start.33 = (bf16[128,512]{1,0:T(8,128)(2,1)S(1)}, bf16[128,512]{1,0:T(8,128)(2,1)S(1)}, u32[]{:S(2)}, u32[]{:S(2)}) collective-permute-start(bf16[128,512]{1,0:T(8,128)(2,1)S(1)} %fusion.1.refs_0_), channel_id=1, source_target_pairs={{0,120},{8,0},{16,8},{24,16},{32,24},{40,32},{48,40},{56,48},{64,5... | collective-permute-start | bytes 393224 | tf_op jit(solution)/shard_map/ppermute | solution.py:475
where the time goes:
time: 203 us
  starting transfers between devices  86.4 us (43%)
  waiting for transfers between devices  72.2 us (36%)
  Pallas kernels  31.2 us (15%)
  blocking collectives  10.8 us (5%)
    ppermute x12, waiting for transfers between devices, along(): return lax.ppermute(x, 'tp', [(i, (i + step) % n) for i in range(n)])  31.7 us
    ppermute x8, starting transfers between devices, across(): lax.ppermute(x, 'tp', [(i, ROUNDS * (i // ROUNDS ^ flip) + i % ROUNDS) fo...  26.3 us
    ppermute x14, waiting for transfers between devices, to_chip(): return lax.ppermute(x, 'dp', [(d, (d + 2 * step) % n) for d in range(n)])  23.9 us
    ppermute x2, starting transfers between devices, to_core(): return lax.ppermute(x, 'dp', [(d, d ^ 1) for d in range(n)])  22.2 us
    ppermute x12, starting transfers between devices, along(): return lax.ppermute(x, 'tp', [(i, (i + step) % n) for i in range(n)])  21.6 us
    ppermute x8, waiting for transfers between devices, across(): lax.ppermute(x, 'tp', [(i, ROUNDS * (i // ROUNDS ^ flip) + i % ROUNDS) fo...  16.6 us
    ppermute x14, starting transfers between devices, to_chip(): return lax.ppermute(x, 'dp', [(d, (d + 2 * step) % n) for d in range(n)])  16.4 us
    all_gather x2, blocking collectives, dp_gather(): return lax.all_gather(near, 'dp', axis_index_groups=pairs, tiled=True)  10.8 us
  transfers between devices with their start and end apart: 36, of which 27 were waited for; matrix products, arithmetic and copies ran while one was open for 0% of the time, Pallas kernels for 8%

commit v1 on v0

--- a/solution.py
+++ b/solution.py
@@ -397,7 +397,7 @@
     i = 0
     for g in g_refs:
         for b in range(g.shape[0]):
-            chosen = (ids == where_ref[pl.ds(meta[16 + i], 1), :]).astype(F32).astype(BF)
+            chosen = (ids == where_ref[pl.ds(meta[i], 1), :]).astype(F32).astype(BF)
             gathered = gathered + dot(chosen, g[b])
             i += 1
     y = dot(gathered.astype(BF), c_ref[0])
@@ -497,11 +497,9 @@
 
 
 def dp_gather(g):
-    n = lax.axis_size("dp")
     far = to_chip(g, -2)
     near = jnp.stack([g, to_chip(g, -1), far, to_chip(g, 1)])
-    pairs = [[d, d + 1] for d in range(0, n, 2)]
-    return lax.all_gather(near, "dp", axis_index_groups=pairs, tiled=True)
+    return near, to_core(near)
 
 
 def tp_sum(parts, x_own, update):
@@ -591,7 +589,7 @@
         if layer == 0:
             where = call_plan(steps, dp, side)
             x_own = call_own_rows(tp, meta, where, x, live_rows)
-        sums = call_close(tp, metas[layer], where, [dp_gather(g)], closing_projector, live_rows)
+        sums = call_close(tp, metas[layer], where, dp_gather(g), closing_projector, live_rows)
 
         def update(own, total):
             total, keys = lax.optimization_barrier((total, wk))

time: 203 us -> 202 us (level)
  the two profiles are of different devices: /device:TPU:33 before, /device:TPU:40 now
where the time goes in v1:
time: 202 us; the launch traced here: 200 us
  starting transfers between devices  87.8 us (43%)
  waiting for transfers between devices  78.6 us (39%)
  Pallas kernels  31.1 us (15%)
    ppermute x12, starting transfers between devices, along(): return lax.ppermute(x, 'tp', [(i, (i + step) % n) for i in range(n)])  40 us
    ppermute x14, waiting for transfers between devices, to_chip(): return lax.ppermute(x, 'dp', [(d, (d + 2 * step) % n) for d in range(n)])  28.9 us
    ppermute x12, waiting for transfers between devices, along(): return lax.ppermute(x, 'tp', [(i, (i + step) % n) for i in range(n)])  28.3 us
    ppermute x8, starting transfers between devices, across(): lax.ppermute(x, 'tp', [(i, ROUNDS * (i // ROUNDS ^ flip) + i % ROUNDS) fo...  25.7 us
    ppermute x14, starting transfers between devices, to_chip(): return lax.ppermute(x, 'dp', [(d, (d + 2 * step) % n) for d in range(n)])  21.5 us
    ppermute x8, waiting for transfers between devices, across(): lax.ppermute(x, 'tp', [(i, ROUNDS * (i // ROUNDS ^ flip) + i % ROUNDS) fo...  18.8 us
    pallas_call x2, Pallas kernels, call_project_first(): pl.pallas_call(functools.partial(project_first, layer, lens.shape[0]), gr...  6.24 us
    pallas_call x2, Pallas kernels, call_project_next(): pl.pallas_call(functools.partial(project_next, layer), grid_spec=pltpu.Pr...  5.43 us
  transfers between devices with their start and end apart: 38, of which 31 were waited for; matrix products, arithmetic and copies ran while one was open for 0% of the time, Pallas kernels for 8%

profile of v1, /device:TPU:40, one launch (start us, length us, event | category | flops | bytes accessed | tf_op | source)
XLA Modules:
  0.0 199.9 jit_solution(15065395828396825535)
XLA Ops:
  0.7 3.1 %project_first.3 = bf16[4,2,128,512]{3,2,1,0:T(8,128)(2,1)S(1)} custom-call(s32[32]{0:T(128)S(1)} %get-tuple-element.90.meta, s32[16]{0:T(128)} %lens.7, bf16[1024,512]{1,0:T(8,128)(2,1)} %bitcast.64, bf16[1024,512]{1,0:T(8,128)(2,1)} %bitcast.65, bf16[2,512]{1,0:T(2,128)(2,1)} %refs_4_.6, bf16[2,512,128]{2,1,0:T(8,128)(2,1)} %refs_5_.3, ...), custom_call_target="tpu_custom_call" | custom-call | tf_op jit(solution)/shard_map/project_first/pallas_call | solution.py:136
  4.0 3.1 %project_first.2.refs_0_ = bf16[4,2,128,512]{3,2,1,0:T(8,128)(2,1)S(1)} custom-call(s32[32]{0:T(128)S(1)} %get-tuple-element.91.meta, s32[16]{0:T(128)} %lens.7, bf16[1024,512]{1,0:T(8,128)(2,1)} %bitcast.66, bf16[1024,512]{1,0:T(8,128)(2,1)} %bitcast.67, bf16[2,512]{1,0:T(2,128)(2,1)} %refs_4_.6, bf16[2,512,128]{2,1,0:T(8,128)(2,1)} %refs_5_.3, ...), custom_call_target="tpu_custom_call" | custom-call | tf_op jit(solution)/shard_map/project_first/pallas_call | solution.py:136
  7.3 3.3 %collective-permute-start.3 = (bf16[128,512]{1,0:T(8,128)(2,1)S(1)}, bf16[128,512]{1,0:T(8,128)(2,1)S(1)}, u32[]{:S(2)}, u32[]{:S(2)}) collective-permute-start(bf16[128,512]{1,0:T(8,128)(2,1)S(1)} %get-tuple-element.77), channel_id=1, source_target_pairs={{0,6},{1,7},{2,0},{3,1},{4,2},{5,3},{6,4},{7,5},{8,14},{9,15},{10,... | collective-permute-start | bytes 393224 | tf_op jit(solution)/shard_map/ppermute | solution.py:465
  10.6 3.5 %collective-permute-done.3 = bf16[128,512]{1,0:T(8,128)(2,1)S(1)} collective-permute-done((bf16[128,512]{1,0:T(8,128)(2,1)S(1)}, bf16[128,512]{1,0:T(8,128)(2,1)S(1)}, u32[]{:S(2)}, u32[]{:S(2)}) %collective-permute-start.3) | collective-permute-done | bytes 131104 | tf_op jit(solution)/shard_map/ppermute | solution.py:465
  14.0 3.4 %collective-permute-done.1 = bf16[128,512]{1,0:T(8,128)(2,1)S(1)} collective-permute-done((bf16[128,512]{1,0:T(8,128)(2,1)S(1)}, bf16[128,512]{1,0:T(8,128)(2,1)S(1)}, u32[]{:S(2)}, u32[]{:S(2)}) %collective-permute-start.1) | collective-permute-done | bytes 131104 | tf_op jit(solution)/shard_map/ppermute | solution.py:465
  17.8 3.3 %collective-permute-start.4 = (bf16[2,128,512]{2,1,0:T(8,128)(2,1)S(1)}, bf16[2,128,512]{2,1,0:T(8,128)(2,1)S(1)}, u32[]{:S(2)}, u32[]{:S(2)}) collective-permute-start(bf16[2,128,512]{2,1,0:T(8,128)(2,1)S(1)} %pad_maximum_fusion.1), channel_id=1, source_target_pairs={{0,6},{1,7},{2,0},{3,1},{4,2},{5,3},{6,4},{7,5},{8,14},{9,15},{10,... | collective-permute-start | bytes 786440 | tf_op jit(solution)/shard_map/ppermute | solution.py:465
  21.3 1.6 load_state.2.refs_7_.state_ref
  22.9 3.7 %collective-permute-done.2.refs_2_ = bf16[2,128,512]{2,1,0:T(8,128)(2,1)S(1)} collective-permute-done((bf16[2,128,512]{2,1,0:T(8,128)(2,1)S(1)}, bf16[2,128,512]{2,1,0:T(8,128)(2,1)S(1)}, u32[]{:S(2)}, u32[]{:S(2)}) %collective-permute-start.2) | collective-permute-done | bytes 262176 | tf_op jit(solution)/shard_map/ppermute | solution.py:465
  26.6 1.3 recur.2
  28.1 4.5 %collective-permute-start.6 = (bf16[128,256]{1,0:T(8,128)(2,1)S(1)}, bf16[128,256]{1,0:T(8,128)(2,1)S(1)}, u32[]{:S(2)}, u32[]{:S(2)}) collective-permute-start(bf16[128,256]{1,0:T(8,128)(2,1)S(1)} %get-tuple-element.36), channel_id=1, source_target_pairs={{0,4},{1,5},{2,6},{3,7},{4,0},{5,1},{6,2},{7,3},{8,12},{9,13},{10,... | collective-permute-start | bytes 196616 | tf_op jit(solution)/shard_map/ppermute | solution.py:465
  32.6 1.0 collective-permute-done.7
  33.6 1.9 collective-permute-done.6
  35.5 1.3 collective-permute-done.5
  37.4 1.1 collective-permute-done.8.refs_1_
  38.5 1.7 close.2
  40.2 5.1 %collective-permute-start.9 = (bf16[128,512]{1,0:T(8,128)(2,1)S(1)}, bf16[128,512]{1,0:T(8,128)(2,1)S(1)}, u32[]{:S(2)}, u32[]{:S(2)}) collective-permute-start(bf16[128,512]{1,0:T(8,128)(2,1)S(1)} %get-tuple-element.38), channel_id=1, source_target_pairs={{0,16},{8,24},{16,32},{24,40},{32,48},{40,56},{48,64},{56,72},{64,... | collective-permute-start | bytes 393224 | tf_op jit(solution)/shard_map/ppermute | solution.py:475
  45.3 2.8 %collective-permute-start.10 = (bf16[128,512]{1,0:T(8,128)(2,1)S(1)}, bf16[128,512]{1,0:T(8,128)(2,1)S(1)}, u32[]{:S(2)}, u32[]{:S(2)}) collective-permute-start(bf16[128,512]{1,0:T(8,128)(2,1)S(1)} %get-tuple-element.39), channel_id=1, source_target_pairs={{0,8},{8,16},{16,24},{24,32},{32,40},{40,48},{48,56},{56,64},{64,7... | collective-permute-start | bytes 393224 | tf_op jit(solution)/shard_map/ppermute | solution.py:475
  48.1 15.1 %collective-permute-start.11 = (bf16[128,512]{1,0:T(8,128)(2,1)S(1)}, bf16[128,512]{1,0:T(8,128)(2,1)S(1)}, u32[]{:S(2)}, u32[]{:S(2)}) collective-permute-start(bf16[128,512]{1,0:T(8,128)(2,1)S(1)} %get-tuple-element.40), channel_id=1, source_target_pairs={{0,120},{8,0},{16,8},{24,16},{32,24},{40,32},{48,40},{56,48},{64,5... | collective-permute-start | bytes 393224 | tf_op jit(solution)/shard_map/ppermute | solution.py:475
  63.1 5.2 %collective-permute-done.9 = bf16[128,512]{1,0:T(8,128)(2,1)S(1)} collective-permute-done((bf16[128,512]{1,0:T(8,128)(2,1)S(1)}, bf16[128,512]{1,0:T(8,128)(2,1)S(1)}, u32[]{:S(2)}, u32[]{:S(2)}) %collective-permute-start.9) | collective-permute-done | bytes 131104 | tf_op jit(solution)/shard_map/ppermute | solution.py:475
  68.4 3.3 %collective-permute-done.10 = bf16[128,512]{1,0:T(8,128)(2,1)S(1)} collective-permute-done((bf16[128,512]{1,0:T(8,128)(2,1)S(1)}, bf16[128,512]{1,0:T(8,128)(2,1)S(1)}, u32[]{:S(2)}, u32[]{:S(2)}) %collective-permute-start.10) | collective-permute-done | bytes 131104 | tf_op jit(solution)/shard_map/ppermute | solution.py:475
  72.0 3.5 %collective-permute-start.14 = (bf16[128,256]{1,0:T(8,128)(2,1)S(1)}, bf16[128,256]{1,0:T(8,128)(2,1)S(1)}, u32[]{:S(2)}, u32[]{:S(2)}) collective-permute-start(bf16[128,256]{1,0:T(8,128)(2,1)S(1)} %get-tuple-element.89), channel_id=1, source_target_pairs={{0,96},{8,104},{16,112},{24,120},{32,64},{40,72},{48,80},{56,88},{... | collective-permute-start | bytes 196616 | tf_op jit(solution)/shard_map/ppermute | solution.py:480
  75.4 0.9 own_rows.1
  76.5 2.6 %update_state.2.refs_0_ = f32[2,16,128,256]{3,2,1,0:T(8,128)} custom-call(bf16[128,128]{1,0:T(8,128)(2,1)S(1)} %get-tuple-element.42.wk_ref, bf16[128,256]{1,0:T(8,128)(2,1)S(1)} %get-tuple-element.43.v_ref, f32[16,1,128]{2,1,0:T(1,128)S(1)} %get-tuple-element.44.end_ref, f32[16,128,256]{2,1,0:T(8,128)S(1)} %load_state.2.refs_7_.state_ref), custom_call_target="tpu_custom_call" | custom-call | tf_op jit(solution)/shard_map/update_state/pallas_call | solution.py:371
  79.1 1.1 collective-permute-done.12
  80.2 1.2 collective-permute-done.14
  81.4 3.3 %collective-permute-start.13 = (bf16[128,256]{1,0:T(8,128)(2,1)S(1)}, bf16[128,256]{1,0:T(8,128)(2,1)S(1)}, u32[]{:S(2)}, u32[]{:S(2)}) collective-permute-start(bf16[128,256]{1,0:T(8,128)(2,1)S(1)} %get-tuple-element.86), channel_id=1, source_target_pairs={{0,96},{8,104},{16,112},{24,120},{32,64},{40,72},{48,80},{56,88},{... | collective-permute-start | bytes 196616 | tf_op jit(solution)/shard_map/ppermute | solution.py:480
  84.7 4.8 %collective-permute-start.15 = (bf16[128,256]{1,0:T(8,128)(2,1)S(1)}, bf16[128,256]{1,0:T(8,128)(2,1)S(1)}, u32[]{:S(2)}, u32[]{:S(2)}) collective-permute-start(bf16[128,256]{1,0:T(8,128)(2,1)S(1)} %get-tuple-element.87), channel_id=1, source_target_pairs={{0,32},{8,40},{16,48},{24,56},{32,0},{40,8},{48,16},{56,24},{64,96... | collective-permute-start | bytes 196616 | tf_op jit(solution)/shard_map/ppermute | solution.py:480
  89.7 4.1 %collective-permute-done.15 = bf16[128,256]{1,0:T(8,128)(2,1)S(1)} collective-permute-done((bf16[128,256]{1,0:T(8,128)(2,1)S(1)}, bf16[128,256]{1,0:T(8,128)(2,1)S(1)}, u32[]{:S(2)}, u32[]{:S(2)}) %collective-permute-start.15) | collective-permute-done | bytes 65568 | tf_op jit(solution)/shard_map/ppermute | solution.py:480
  93.9 3.5 %collective-permute-start.18 = (bf16[128,512]{1,0:T(8,128)(2,1)S(1)}, bf16[128,512]{1,0:T(8,128)(2,1)S(1)}, u32[]{:S(2)}, u32[]{:S(2)}) collective-permute-start(bf16[128,512]{1,0:T(8,128)(2,1)S(1)} %fusion.refs_0_), channel_id=1, source_target_pairs={{0,112},{8,120},{16,0},{24,8},{32,16},{40,24},{48,32},{56,40},{64,... | collective-permute-start | bytes 393224 | tf_op jit(solution)/shard_map/ppermute | solution.py:475
  97.5 1.6 collective-permute-start.17
  99.1 1.6 collective-permute-start.16
  100.7 3.8 %collective-permute-done.18.refs_3_ = bf16[128,512]{1,0:T(8,128)(2,1)S(1)} collective-permute-done((bf16[128,512]{1,0:T(8,128)(2,1)S(1)}, bf16[128,512]{1,0:T(8,128)(2,1)S(1)}, u32[]{:S(2)}, u32[]{:S(2)}) %collective-permute-start.18) | collective-permute-done | bytes 131104 | tf_op jit(solution)/shard_map/ppermute | solution.py:475
  104.6 1.8 collective-permute-done.16.refs_1_
  106.4 2.7 %project_next.3 = bf16[4,2,128,512]{3,2,1,0:T(8,128)(2,1)S(1)} custom-call(s32[32]{0:T(128)S(1)} %get-tuple-element.90.meta, f32[8,128]{1,0:T(8,128)S(1)} %plan.1.where_ref, bf16[128,512]{1,0:T(8,128)(2,1)S(1)} %fusion.refs_0_, bf16[128,512]{1,0:T(8,128)(2,1)S(1)} %collective-permute-done.16.refs_1_, bf16[128,512]{1,0:T(8,128)(2,1)S(1)} %collective-permute-done.17.refs_2_, ...), custom_call_target="tpu_custom_call" | custom-call | tf_op jit(solution)/shard_map/project_next/pallas_call | solution.py:160
  109.2 2.7 %project_next.2.refs_0_ = bf16[4,2,128,512]{3,2,1,0:T(8,128)(2,1)S(1)} custom-call(s32[32]{0:T(128)S(1)} %get-tuple-element.68.meta, f32[8,128]{1,0:T(8,128)S(1)} %plan.1.where_ref, bf16[128,512]{1,0:T(8,128)(2,1)S(1)} %fusion.refs_0_, bf16[128,512]{1,0:T(8,128)(2,1)S(1)} %collective-permute-done.16.refs_1_, ...), custom_call_target="tpu_custom_call" | custom-call | tf_op jit(solution)/shard_map/project_next/pallas_call | solution.py:160
  112.1 1.3 collective-permute-start.22
  114.3 3.9 %collective-permute-done.22 = bf16[128,512]{1,0:T(8,128)(2,1)S(1)} collective-permute-done((bf16[128,512]{1,0:T(8,128)(2,1)S(1)}, bf16[128,512]{1,0:T(8,128)(2,1)S(1)}, u32[]{:S(2)}, u32[]{:S(2)}) %collective-permute-start.22) | collective-permute-done | bytes 131104 | tf_op jit(solution)/shard_map/ppermute | solution.py:465
  118.1 2.1 %collective-permute-done.20 = bf16[128,512]{1,0:T(8,128)(2,1)S(1)} collective-permute-done((bf16[128,512]{1,0:T(8,128)(2,1)S(1)}, bf16[128,512]{1,0:T(8,128)(2,1)S(1)}, u32[]{:S(2)}, u32[]{:S(2)}) %collective-permute-start.20) | collective-permute-done | bytes 131104 | tf_op jit(solution)/shard_map/ppermute | solution.py:465
  120.5 3.3 %collective-permute-start.23 = (bf16[2,128,512]{2,1,0:T(8,128)(2,1)S(1)}, bf16[2,128,512]{2,1,0:T(8,128)(2,1)S(1)}, u32[]{:S(2)}, u32[]{:S(2)}) collective-permute-start(bf16[2,128,512]{2,1,0:T(8,128)(2,1)S(1)} %pad_maximum_fusion.4), channel_id=1, source_target_pairs={{0,6},{1,7},{2,0},{3,1},{4,2},{5,3},{6,4},{7,5},{8,14},{9,15},{10,... | collective-permute-start | bytes 786440 | tf_op jit(solution)/shard_map/ppermute | solution.py:465
  123.9 1.6 load_state.3.refs_7_.state_ref
  125.5 3.8 %collective-permute-done.21.refs_2_ = bf16[2,128,512]{2,1,0:T(8,128)(2,1)S(1)} collective-permute-done((bf16[2,128,512]{2,1,0:T(8,128)(2,1)S(1)}, bf16[2,128,512]{2,1,0:T(8,128)(2,1)S(1)}, u32[]{:S(2)}, u32[]{:S(2)}) %collective-permute-start.21) | collective-permute-done | bytes 262176 | tf_op jit(solution)/shard_map/ppermute | solution.py:465
  129.2 1.8 recur.3
  131.0 4.6 %collective-permute-start.25 = (bf16[128,256]{1,0:T(8,128)(2,1)S(1)}, bf16[128,256]{1,0:T(8,128)(2,1)S(1)}, u32[]{:S(2)}, u32[]{:S(2)}) collective-permute-start(bf16[128,256]{1,0:T(8,128)(2,1)S(1)} %get-tuple-element.50), channel_id=1, source_target_pairs={{0,4},{1,5},{2,6},{3,7},{4,0},{5,1},{6,2},{7,3},{8,12},{9,13},{10,... | collective-permute-start | bytes 196616 | tf_op jit(solution)/shard_map/ppermute | solution.py:465
  135.6 0.9 collective-permute-done.26
  136.5 2.0 %collective-permute-done.25 = bf16[128,256]{1,0:T(8,128)(2,1)S(1)} collective-permute-done((bf16[128,256]{1,0:T(8,128)(2,1)S(1)}, bf16[128,256]{1,0:T(8,128)(2,1)S(1)}, u32[]{:S(2)}, u32[]{:S(2)}) %collective-permute-start.25) | collective-permute-done | bytes 65568 | tf_op jit(solution)/shard_map/ppermute | solution.py:465
  138.5 1.3 collective-permute-done.24
  140.0 1.5 collective-permute-done.27.refs_1_
  141.5 1.6 close.3
  143.2 1.8 collective-permute-start.28
  145.0 2.4 %collective-permute-start.29 = (bf16[128,512]{1,0:T(8,128)(2,1)S(1)}, bf16[128,512]{1,0:T(8,128)(2,1)S(1)}, u32[]{:S(2)}, u32[]{:S(2)}) collective-permute-start(bf16[128,512]{1,0:T(8,128)(2,1)S(1)} %get-tuple-element.53), channel_id=1, source_target_pairs={{0,8},{8,16},{16,24},{24,32},{32,40},{40,48},{48,56},{56,64},{64,7... | collective-permute-start | bytes 393224 | tf_op jit(solution)/shard_map/ppermute | solution.py:475
  148.2 6.4 %collective-permute-done.28 = bf16[128,512]{1,0:T(8,128)(2,1)S(1)} collective-permute-done((bf16[128,512]{1,0:T(8,128)(2,1)S(1)}, bf16[128,512]{1,0:T(8,128)(2,1)S(1)}, u32[]{:S(2)}, u32[]{:S(2)}) %collective-permute-start.28) | collective-permute-done | bytes 131104 | tf_op jit(solution)/shard_map/ppermute | solution.py:475
  155.5 4.1 %collective-permute-start.31 = (bf16[128,256]{1,0:T(8,128)(2,1)S(1)}, bf16[128,256]{1,0:T(8,128)(2,1)S(1)}, u32[]{:S(2)}, u32[]{:S(2)}) collective-permute-start(bf16[128,256]{1,0:T(8,128)(2,1)S(1)} %get-tuple-element.84), channel_id=1, source_target_pairs={{0,32},{8,40},{16,48},{24,56},{32,0},{40,8},{48,16},{56,24},{64,96... | collective-permute-start | bytes 196616 | tf_op jit(solution)/shard_map/ppermute | solution.py:480
  159.6 4.5 %collective-permute-start.33 = (bf16[128,256]{1,0:T(8,128)(2,1)S(1)}, bf16[128,256]{1,0:T(8,128)(2,1)S(1)}, u32[]{:S(2)}, u32[]{:S(2)}) collective-permute-start(bf16[128,256]{1,0:T(8,128)(2,1)S(1)} %get-tuple-element.85), channel_id=1, source_target_pairs={{0,96},{8,104},{16,112},{24,120},{32,64},{40,72},{48,80},{56,88},{... | collective-permute-start | bytes 196616 | tf_op jit(solution)/shard_map/ppermute | solution.py:480
  164.1 2.6 %update_state.3 = f32[2,16,128,256]{3,2,1,0:T(8,128)} custom-call(bf16[128,128]{1,0:T(8,128)(2,1)S(1)} %get-tuple-element.56.wk_ref, bf16[128,256]{1,0:T(8,128)(2,1)S(1)} %get-tuple-element.57.v_ref, f32[16,1,128]{2,1,0:T(1,128)S(1)} %get-tuple-element.58.end_ref, f32[16,128,256]{2,1,0:T(8,128)S(1)} %load_state.3.refs_7_.state_ref, ...), custom_call_target="tpu_custom_call", output_to_operand_aliasing={{}: (4, {})} | custom-call | tf_op jit(solution)/shard_map/update_state/pallas_call | solution.py:371
  167.4 1.6 collective-permute-done.33
  169.0 5.0 %collective-permute-start.32 = (bf16[128,256]{1,0:T(8,128)(2,1)S(1)}, bf16[128,256]{1,0:T(8,128)(2,1)S(1)}, u32[]{:S(2)}, u32[]{:S(2)}) collective-permute-start(bf16[128,256]{1,0:T(8,128)(2,1)S(1)} %get-tuple-element.82), channel_id=1, source_target_pairs={{0,96},{8,104},{16,112},{24,120},{32,64},{40,72},{48,80},{56,88},{... | collective-permute-start | bytes 196616 | tf_op jit(solution)/shard_map/ppermute | solution.py:480
  174.3 3.9 %collective-permute-done.32 = bf16[128,256]{1,0:T(8,128)(2,1)S(1)} collective-permute-done((bf16[128,256]{1,0:T(8,128)(2,1)S(1)}, bf16[128,256]{1,0:T(8,128)(2,1)S(1)}, u32[]{:S(2)}, u32[]{:S(2)}) %collective-permute-start.32) | collective-permute-done | bytes 65568 | tf_op jit(solution)/shard_map/ppermute | solution.py:480
  178.3 6.1 %collective-permute-done.34 = bf16[128,256]{1,0:T(8,128)(2,1)S(1)} collective-permute-done((bf16[128,256]{1,0:T(8,128)(2,1)S(1)}, bf16[128,256]{1,0:T(8,128)(2,1)S(1)}, u32[]{:S(2)}, u32[]{:S(2)}) %collective-permute-start.34) | collective-permute-done | bytes 65568 | tf_op jit(solution)/shard_map/ppermute | solution.py:480
  184.4 2.0 %collective-permute-start.37 = (bf16[128,512]{1,0:T(8,128)(2,1)S(1)}, bf16[128,512]{1,0:T(8,128)(2,1)S(1)}, u32[]{:S(2)}, u32[]{:S(2)}) collective-permute-start(bf16[128,512]{1,0:T(8,128)(2,1)S(1)} %fusion.1.refs_0_), channel_id=1, source_target_pairs={{0,112},{8,120},{16,0},{24,8},{32,16},{40,24},{48,32},{56,40},{64,... | collective-permute-start | bytes 393224 | tf_op jit(solution)/shard_map/ppermute | solution.py:475
  186.4 2.2 %collective-permute-start.36 = (bf16[128,512]{1,0:T(8,128)(2,1)S(1)}, bf16[128,512]{1,0:T(8,128)(2,1)S(1)}, u32[]{:S(2)}, u32[]{:S(2)}) collective-permute-start(bf16[128,512]{1,0:T(8,128)(2,1)S(1)} %fusion.1.refs_0_), channel_id=1, source_target_pairs={{0,8},{8,16},{16,24},{24,32},{32,40},{40,48},{48,56},{56,64},{64,7... | collective-permute-start | bytes 393224 | tf_op jit(solution)/shard_map/ppermute | solution.py:475
  188.6 1.1 collective-permute-start.35
  189.7 2.8 %collective-permute-done.37.refs_3_ = bf16[128,512]{1,0:T(8,128)(2,1)S(1)} collective-permute-done((bf16[128,512]{1,0:T(8,128)(2,1)S(1)}, bf16[128,512]{1,0:T(8,128)(2,1)S(1)}, u32[]{:S(2)}, u32[]{:S(2)}) %collective-permute-start.37) | collective-permute-done | bytes 131104 | tf_op jit(solution)/shard_map/ppermute | solution.py:475
  192.6 4.0 %collective-permute-done.35.refs_1_ = bf16[128,512]{1,0:T(8,128)(2,1)S(1)} collective-permute-done((bf16[128,512]{1,0:T(8,128)(2,1)S(1)}, bf16[128,512]{1,0:T(8,128)(2,1)S(1)}, u32[]{:S(2)}, u32[]{:S(2)}) %collective-permute-start.35) | collective-permute-done | bytes 131104 | tf_op jit(solution)/shard_map/ppermute | solution.py:475
  196.6 3.3 %finish.1 = bf16[1024,512]{1,0:T(8,128)(2,1)} custom-call(s32[32]{0:T(128)S(1)} %get-tuple-element.69.meta, f32[8,128]{1,0:T(8,128)S(1)} %plan.1.where_ref, bf16[128,512]{1,0:T(8,128)(2,1)S(1)} %fusion.1.refs_0_, bf16[128,512]{1,0:T(8,128)(2,1)S(1)} %collective-permute-done.35.refs_1_, bf16[128,512]{1,0:T(8,128)(2,1)S(1)} %collective-permute-done.36.refs_2_, ...), custom_call_target="tpu_custom_call" | custom-call | tf_op jit(solution)/shard_map/finish/pallas_call | solution.py:182
  (79 shorter events, 6.6 us)
Async XLA Ops:
  3.8 3.3 %collective-permute-start = (bf16[4,2,128,512]{3,2,1,0:T(8,128)(2,1)S(1)}, bf16[4,2,128,512]{3,2,1,0:T(8,128)(2,1)S(1)}, u32[]{:S(2)}, u32[]{:S(2)}) collective-permute-start(bf16[4,2,128,512]{3,2,1,0:T(8,128)(2,1)S(1)} %project_first.3), channel_id=1, source_target_pairs={{0,1},{1,0},{2,3},{3,2},{4,5},{5,4},{6,7},{7,6},{8,9},{9,8},{10,11... | collective-permute-start | bytes 3145736 | tf_op jit(solution)/shard_map/ppermute | solution.py:470
  4.0 17.1 %copy-start.11 = (f32[16,8,1]{0,2,1:T(1,128)S(1)}, f32[16,8,1]{0,2,1:T(1,128)}, u32[]{:S(2)}) copy-start(f32[16,8,1]{0,2,1:T(1,128)} %param.22) | copy-start | bytes 1540
  7.3 6.8 %collective-permute-start.3 = (bf16[128,512]{1,0:T(8,128)(2,1)S(1)}, bf16[128,512]{1,0:T(8,128)(2,1)S(1)}, u32[]{:S(2)}, u32[]{:S(2)}) collective-permute-start(bf16[128,512]{1,0:T(8,128)(2,1)S(1)} %get-tuple-element.77), channel_id=1, source_target_pairs={{0,6},{1,7},{2,0},{3,1},{4,2},{5,3},{6,4},{7,5},{8,14},{9,15},{10,... | collective-permute-start | bytes 393224 | tf_op jit(solution)/shard_map/ppermute | solution.py:465
  10.5 16.1 %copy-start.8 = (s32[16]{0:T(128)S(1)}, s32[16]{0:T(128)}, u32[]{:S(2)}) copy-start(s32[16]{0:T(128)} %lens.7) | copy-start | bytes 196
  10.5 16.1 %copy-start.9 = (f32[2,128]{1,0:T(2,128)S(1)}, f32[2,128]{1,0:T(2,128)}, u32[]{:S(2)}) copy-start(f32[2,128]{1,0:T(2,128)} %refs_4_.7) | copy-start | bytes 3076
  10.5 16.1 %copy-start.10 = (bf16[2,256]{1,0:T(2,128)(2,1)S(1)}, bf16[2,256]{1,0:T(2,128)(2,1)}, u32[]{:S(2)}) copy-start(bf16[2,256]{1,0:T(2,128)(2,1)} %refs_6_.7) | copy-start | bytes 3076
  10.5 6.9 %collective-permute-start.1 = (bf16[128,512]{1,0:T(8,128)(2,1)S(1)}, bf16[128,512]{1,0:T(8,128)(2,1)S(1)}, u32[]{:S(2)}, u32[]{:S(2)}) collective-permute-start(bf16[128,512]{1,0:T(8,128)(2,1)S(1)} %get-tuple-element.79), channel_id=1, source_target_pairs={{0,2},{1,3},{2,4},{3,5},{4,6},{5,7},{6,0},{7,1},{8,10},{9,11},{10,... | collective-permute-start | bytes 393224 | tf_op jit(solution)/shard_map/ppermute | solution.py:465
  17.6 9.0 %collective-permute-start.2 = (bf16[2,128,512]{2,1,0:T(8,128)(2,1)S(1)}, bf16[2,128,512]{2,1,0:T(8,128)(2,1)S(1)}, u32[]{:S(2)}, u32[]{:S(2)}) collective-permute-start(bf16[2,128,512]{2,1,0:T(8,128)(2,1)S(1)} %pad_maximum_fusion), channel_id=1, source_target_pairs={{0,2},{1,3},{2,4},{3,5},{4,6},{5,7},{6,0},{7,1},{8,10},{9,11},{10,... | collective-permute-start | bytes 786440 | tf_op jit(solution)/shard_map/ppermute | solution.py:465
  17.8 8.8 %collective-permute-start.4 = (bf16[2,128,512]{2,1,0:T(8,128)(2,1)S(1)}, bf16[2,128,512]{2,1,0:T(8,128)(2,1)S(1)}, u32[]{:S(2)}, u32[]{:S(2)}) collective-permute-start(bf16[2,128,512]{2,1,0:T(8,128)(2,1)S(1)} %pad_maximum_fusion.1), channel_id=1, source_target_pairs={{0,6},{1,7},{2,0},{3,1},{4,2},{5,3},{6,4},{7,5},{8,14},{9,15},{10,... | collective-permute-start | bytes 786440 | tf_op jit(solution)/shard_map/ppermute | solution.py:465
  22.9 15.7 %copy-start.6 = (bf16[2,256,512]{2,1,0:T(8,128)(2,1)S(1)}, bf16[2,256,512]{2,1,0:T(8,128)(2,1)}, u32[]{:S(2)}) copy-start(bf16[2,256,512]{2,1,0:T(8,128)(2,1)} %refs_2_.3) | copy-start | bytes 1572868
  22.9 52.5 %copy-start = (bf16[128,8,512]{2,1,0:T(8,128)(2,1)S(1)}, bf16[128,8,512]{2,1,0:T(8,128)(2,1)}, u32[]{:S(2)}) copy-start(bf16[128,8,512]{2,1,0:T(8,128)(2,1)} %param.13) | copy-start | bytes 3145732
  27.9 5.7 %collective-permute-start.7 = (bf16[128,256]{1,0:T(8,128)(2,1)S(1)}, bf16[128,256]{1,0:T(8,128)(2,1)S(1)}, u32[]{:S(2)}, u32[]{:S(2)}) collective-permute-start(bf16[128,256]{1,0:T(8,128)(2,1)S(1)} %get-tuple-element.36), channel_id=1, source_target_pairs={{0,2},{1,3},{2,4},{3,5},{4,6},{5,7},{6,0},{7,1},{8,10},{9,11},{10,... | collective-permute-start | bytes 196616 | tf_op jit(solution)/shard_map/ppermute | solution.py:465
  28.1 7.5 %collective-permute-start.6 = (bf16[128,256]{1,0:T(8,128)(2,1)S(1)}, bf16[128,256]{1,0:T(8,128)(2,1)S(1)}, u32[]{:S(2)}, u32[]{:S(2)}) collective-permute-start(bf16[128,256]{1,0:T(8,128)(2,1)S(1)} %get-tuple-element.36), channel_id=1, source_target_pairs={{0,4},{1,5},{2,6},{3,7},{4,0},{5,1},{6,2},{7,3},{8,12},{9,13},{10,... | collective-permute-start | bytes 196616 | tf_op jit(solution)/shard_map/ppermute | solution.py:465
  32.6 4.3 %collective-permute-start.5 = (bf16[128,256]{1,0:T(8,128)(2,1)S(1)}, bf16[128,256]{1,0:T(8,128)(2,1)S(1)}, u32[]{:S(2)}, u32[]{:S(2)}) collective-permute-start(bf16[128,256]{1,0:T(8,128)(2,1)S(1)} %get-tuple-element.36), channel_id=1, source_target_pairs={{0,6},{1,7},{2,0},{3,1},{4,2},{5,3},{6,4},{7,5},{8,14},{9,15},{10,... | collective-permute-start | bytes 196616 | tf_op jit(solution)/shard_map/ppermute | solution.py:465
  36.9 1.7 collective-permute-start.8
  40.2 28.2 %collective-permute-start.9 = (bf16[128,512]{1,0:T(8,128)(2,1)S(1)}, bf16[128,512]{1,0:T(8,128)(2,1)S(1)}, u32[]{:S(2)}, u32[]{:S(2)}) collective-permute-start(bf16[128,512]{1,0:T(8,128)(2,1)S(1)} %get-tuple-element.38), channel_id=1, source_target_pairs={{0,16},{8,24},{16,32},{24,40},{32,48},{40,56},{48,64},{56,72},{64,... | collective-permute-start | bytes 393224 | tf_op jit(solution)/shard_map/ppermute | solution.py:475
  45.3 26.4 %collective-permute-start.10 = (bf16[128,512]{1,0:T(8,128)(2,1)S(1)}, bf16[128,512]{1,0:T(8,128)(2,1)S(1)}, u32[]{:S(2)}, u32[]{:S(2)}) collective-permute-start(bf16[128,512]{1,0:T(8,128)(2,1)S(1)} %get-tuple-element.39), channel_id=1, source_target_pairs={{0,8},{8,16},{16,24},{24,32},{32,40},{40,48},{48,56},{56,64},{64,7... | collective-permute-start | bytes 393224 | tf_op jit(solution)/shard_map/ppermute | solution.py:475
  48.1 23.6 %collective-permute-start.11 = (bf16[128,512]{1,0:T(8,128)(2,1)S(1)}, bf16[128,512]{1,0:T(8,128)(2,1)S(1)}, u32[]{:S(2)}, u32[]{:S(2)}) collective-permute-start(bf16[128,512]{1,0:T(8,128)(2,1)S(1)} %get-tuple-element.40), channel_id=1, source_target_pairs={{0,120},{8,0},{16,8},{24,16},{32,24},{40,32},{48,40},{56,48},{64,5... | collective-permute-start | bytes 393224 | tf_op jit(solution)/shard_map/ppermute | solution.py:475
  71.8 8.4 %collective-permute-start.12 = (bf16[128,256]{1,0:T(8,128)(2,1)S(1)}, bf16[128,256]{1,0:T(8,128)(2,1)S(1)}, u32[]{:S(2)}, u32[]{:S(2)}) collective-permute-start(bf16[128,256]{1,0:T(8,128)(2,1)S(1)} %get-tuple-element.88), channel_id=1, source_target_pairs={{0,32},{8,40},{16,48},{24,56},{32,0},{40,8},{48,16},{56,24},{64,96... | collective-permute-start | bytes 196616 | tf_op jit(solution)/shard_map/ppermute | solution.py:480
  72.0 9.4 %collective-permute-start.14 = (bf16[128,256]{1,0:T(8,128)(2,1)S(1)}, bf16[128,256]{1,0:T(8,128)(2,1)S(1)}, u32[]{:S(2)}, u32[]{:S(2)}) collective-permute-start(bf16[128,256]{1,0:T(8,128)(2,1)S(1)} %get-tuple-element.89), channel_id=1, source_target_pairs={{0,96},{8,104},{16,112},{24,120},{32,64},{40,72},{48,80},{56,88},{... | collective-permute-start | bytes 196616 | tf_op jit(solution)/shard_map/ppermute | solution.py:480
  76.4 29.9 %copy-start.1 = (bf16[2,512,256]{2,1,0:T(8,128)(2,1)S(1)}, bf16[2,512,256]{2,1,0:T(8,128)(2,1)}, u32[]{:S(2)}) copy-start(bf16[2,512,256]{2,1,0:T(8,128)(2,1)} %refs_7_.3) | copy-start | bytes 1572868
  76.4 29.9 %copy-start.2 = (bf16[2,512,256]{2,1,0:T(8,128)(2,1)S(1)}, bf16[2,512,256]{2,1,0:T(8,128)(2,1)}, u32[]{:S(2)}) copy-start(bf16[2,512,256]{2,1,0:T(8,128)(2,1)} %refs_8_.3) | copy-start | bytes 1572868
  76.4 29.9 %copy-start.3 = (bf16[2,512,128]{2,1,0:T(8,128)(2,1)S(1)}, bf16[2,512,128]{2,1,0:T(8,128)(2,1)}, u32[]{:S(2)}) copy-start(bf16[2,512,128]{2,1,0:T(8,128)(2,1)} %refs_5_.3) | copy-start | bytes 786436
  76.4 29.9 %copy-start.4 = (bf16[2,512,128]{2,1,0:T(8,128)(2,1)S(1)}, bf16[2,512,128]{2,1,0:T(8,128)(2,1)}, u32[]{:S(2)}) copy-start(bf16[2,512,128]{2,1,0:T(8,128)(2,1)} %refs_6_.6) | copy-start | bytes 786436
  76.4 29.9 %copy-start.5 = (bf16[2,512,128]{2,1,0:T(8,128)(2,1)S(1)}, bf16[2,512,128]{2,1,0:T(8,128)(2,1)}, u32[]{:S(2)}) copy-start(bf16[2,512,128]{2,1,0:T(8,128)(2,1)} %refs_9_.3) | copy-start | bytes 786436
  76.4 29.9 %copy-start.7 = (bf16[2,512]{1,0:T(2,128)(2,1)S(1)}, bf16[2,512]{1,0:T(2,128)(2,1)}, u32[]{:S(2)}) copy-start(bf16[2,512]{1,0:T(2,128)(2,1)} %refs_4_.6) | copy-start | bytes 6148
  81.4 8.3 %collective-permute-start.13 = (bf16[128,256]{1,0:T(8,128)(2,1)S(1)}, bf16[128,256]{1,0:T(8,128)(2,1)S(1)}, u32[]{:S(2)}, u32[]{:S(2)}) collective-permute-start(bf16[128,256]{1,0:T(8,128)(2,1)S(1)} %get-tuple-element.86), channel_id=1, source_target_pairs={{0,96},{8,104},{16,112},{24,120},{32,64},{40,72},{48,80},{56,88},{... | collective-permute-start | bytes 196616 | tf_op jit(solution)/shard_map/ppermute | solution.py:480
  84.7 9.1 %collective-permute-start.15 = (bf16[128,256]{1,0:T(8,128)(2,1)S(1)}, bf16[128,256]{1,0:T(8,128)(2,1)S(1)}, u32[]{:S(2)}, u32[]{:S(2)}) collective-permute-start(bf16[128,256]{1,0:T(8,128)(2,1)S(1)} %get-tuple-element.87), channel_id=1, source_target_pairs={{0,32},{8,40},{16,48},{24,56},{32,0},{40,8},{48,16},{56,24},{64,96... | collective-permute-start | bytes 196616 | tf_op jit(solution)/shard_map/ppermute | solution.py:480
  93.9 10.6 %collective-permute-start.18 = (bf16[128,512]{1,0:T(8,128)(2,1)S(1)}, bf16[128,512]{1,0:T(8,128)(2,1)S(1)}, u32[]{:S(2)}, u32[]{:S(2)}) collective-permute-start(bf16[128,512]{1,0:T(8,128)(2,1)S(1)} %fusion.refs_0_), channel_id=1, source_target_pairs={{0,112},{8,120},{16,0},{24,8},{32,16},{40,24},{48,32},{56,40},{64,... | collective-permute-start | bytes 393224 | tf_op jit(solution)/shard_map/ppermute | solution.py:475
  97.5 7.1 %collective-permute-start.17 = (bf16[128,512]{1,0:T(8,128)(2,1)S(1)}, bf16[128,512]{1,0:T(8,128)(2,1)S(1)}, u32[]{:S(2)}, u32[]{:S(2)}) collective-permute-start(bf16[128,512]{1,0:T(8,128)(2,1)S(1)} %fusion.refs_0_), channel_id=1, source_target_pairs={{0,8},{8,16},{16,24},{24,32},{32,40},{40,48},{48,56},{56,64},{64,7... | collective-permute-start | bytes 393224 | tf_op jit(solution)/shard_map/ppermute | solution.py:475
  99.1 7.2 %collective-permute-start.16 = (bf16[128,512]{1,0:T(8,128)(2,1)S(1)}, bf16[128,512]{1,0:T(8,128)(2,1)S(1)}, u32[]{:S(2)}, u32[]{:S(2)}) collective-permute-start(bf16[128,512]{1,0:T(8,128)(2,1)S(1)} %fusion.refs_0_), channel_id=1, source_target_pairs={{0,120},{8,0},{16,8},{24,16},{32,24},{40,32},{48,40},{56,48},{64,5... | collective-permute-start | bytes 393224 | tf_op jit(solution)/shard_map/ppermute | solution.py:475
  109.1 2.9 %collective-permute-start.19 = (bf16[4,2,128,512]{3,2,1,0:T(8,128)(2,1)S(1)}, bf16[4,2,128,512]{3,2,1,0:T(8,128)(2,1)S(1)}, u32[]{:S(2)}, u32[]{:S(2)}) collective-permute-start(bf16[4,2,128,512]{3,2,1,0:T(8,128)(2,1)S(1)} %project_next.3), channel_id=1, source_target_pairs={{0,1},{1,0},{2,3},{3,2},{4,5},{5,4},{6,7},{7,6},{8,9},{9,8},{10,11... | collective-permute-start | bytes 3145736 | tf_op jit(solution)/shard_map/ppermute | solution.py:470
  112.1 6.0 %collective-permute-start.22 = (bf16[128,512]{1,0:T(8,128)(2,1)S(1)}, bf16[128,512]{1,0:T(8,128)(2,1)S(1)}, u32[]{:S(2)}, u32[]{:S(2)}) collective-permute-start(bf16[128,512]{1,0:T(8,128)(2,1)S(1)} %get-tuple-element.71), channel_id=1, source_target_pairs={{0,6},{1,7},{2,0},{3,1},{4,2},{5,3},{6,4},{7,5},{8,14},{9,15},{10,... | collective-permute-start | bytes 393224 | tf_op jit(solution)/shard_map/ppermute | solution.py:465
  113.4 6.8 %collective-permute-start.20 = (bf16[128,512]{1,0:T(8,128)(2,1)S(1)}, bf16[128,512]{1,0:T(8,128)(2,1)S(1)}, u32[]{:S(2)}, u32[]{:S(2)}) collective-permute-start(bf16[128,512]{1,0:T(8,128)(2,1)S(1)} %get-tuple-element.73), channel_id=1, source_target_pairs={{0,2},{1,3},{2,4},{3,5},{4,6},{5,7},{6,0},{7,1},{8,10},{9,11},{10,... | collective-permute-start | bytes 393224 | tf_op jit(solution)/shard_map/ppermute | solution.py:465
  120.4 8.9 %collective-permute-start.21 = (bf16[2,128,512]{2,1,0:T(8,128)(2,1)S(1)}, bf16[2,128,512]{2,1,0:T(8,128)(2,1)S(1)}, u32[]{:S(2)}, u32[]{:S(2)}) collective-permute-start(bf16[2,128,512]{2,1,0:T(8,128)(2,1)S(1)} %pad_maximum_fusion.3), channel_id=1, source_target_pairs={{0,2},{1,3},{2,4},{3,5},{4,6},{5,7},{6,0},{7,1},{8,10},{9,11},{10,... | collective-permute-start | bytes 786440 | tf_op jit(solution)/shard_map/ppermute | solution.py:465
  120.5 8.7 %collective-permute-start.23 = (bf16[2,128,512]{2,1,0:T(8,128)(2,1)S(1)}, bf16[2,128,512]{2,1,0:T(8,128)(2,1)S(1)}, u32[]{:S(2)}, u32[]{:S(2)}) collective-permute-start(bf16[2,128,512]{2,1,0:T(8,128)(2,1)S(1)} %pad_maximum_fusion.4), channel_id=1, source_target_pairs={{0,6},{1,7},{2,0},{3,1},{4,2},{5,3},{6,4},{7,5},{8,14},{9,15},{10,... | collective-permute-start | bytes 786440 | tf_op jit(solution)/shard_map/ppermute | solution.py:465
  131.0 5.5 %collective-permute-start.26 = (bf16[128,256]{1,0:T(8,128)(2,1)S(1)}, bf16[128,256]{1,0:T(8,128)(2,1)S(1)}, u32[]{:S(2)}, u32[]{:S(2)}) collective-permute-start(bf16[128,256]{1,0:T(8,128)(2,1)S(1)} %get-tuple-element.50), channel_id=1, source_target_pairs={{0,2},{1,3},{2,4},{3,5},{4,6},{5,7},{6,0},{7,1},{8,10},{9,11},{10,... | collective-permute-start | bytes 196616 | tf_op jit(solution)/shard_map/ppermute | solution.py:465
  131.0 7.5 %collective-permute-start.25 = (bf16[128,256]{1,0:T(8,128)(2,1)S(1)}, bf16[128,256]{1,0:T(8,128)(2,1)S(1)}, u32[]{:S(2)}, u32[]{:S(2)}) collective-permute-start(bf16[128,256]{1,0:T(8,128)(2,1)S(1)} %get-tuple-element.50), channel_id=1, source_target_pairs={{0,4},{1,5},{2,6},{3,7},{4,0},{5,1},{6,2},{7,3},{8,12},{9,13},{10,... | collective-permute-start | bytes 196616 | tf_op jit(solution)/shard_map/ppermute | solution.py:465
  135.6 4.3 %collective-permute-start.24 = (bf16[128,256]{1,0:T(8,128)(2,1)S(1)}, bf16[128,256]{1,0:T(8,128)(2,1)S(1)}, u32[]{:S(2)}, u32[]{:S(2)}) collective-permute-start(bf16[128,256]{1,0:T(8,128)(2,1)S(1)} %get-tuple-element.50), channel_id=1, source_target_pairs={{0,6},{1,7},{2,0},{3,1},{4,2},{5,3},{6,4},{7,5},{8,14},{9,15},{10,... | collective-permute-start | bytes 196616 | tf_op jit(solution)/shard_map/ppermute | solution.py:465
  139.9 1.7 collective-permute-start.27
  143.2 11.4 %collective-permute-start.28 = (bf16[128,512]{1,0:T(8,128)(2,1)S(1)}, bf16[128,512]{1,0:T(8,128)(2,1)S(1)}, u32[]{:S(2)}, u32[]{:S(2)}) collective-permute-start(bf16[128,512]{1,0:T(8,128)(2,1)S(1)} %get-tuple-element.52), channel_id=1, source_target_pairs={{0,16},{8,24},{16,32},{24,40},{32,48},{40,56},{48,64},{56,72},{64,... | collective-permute-start | bytes 393224 | tf_op jit(solution)/shard_map/ppermute | solution.py:475
  145.0 10.4 %collective-permute-start.29 = (bf16[128,512]{1,0:T(8,128)(2,1)S(1)}, bf16[128,512]{1,0:T(8,128)(2,1)S(1)}, u32[]{:S(2)}, u32[]{:S(2)}) collective-permute-start(bf16[128,512]{1,0:T(8,128)(2,1)S(1)} %get-tuple-element.53), channel_id=1, source_target_pairs={{0,8},{8,16},{16,24},{24,32},{32,40},{40,48},{48,56},{56,64},{64,7... | collective-permute-start | bytes 393224 | tf_op jit(solution)/shard_map/ppermute | solution.py:475
  147.4 8.0 %collective-permute-start.30 = (bf16[128,512]{1,0:T(8,128)(2,1)S(1)}, bf16[128,512]{1,0:T(8,128)(2,1)S(1)}, u32[]{:S(2)}, u32[]{:S(2)}) collective-permute-start(bf16[128,512]{1,0:T(8,128)(2,1)S(1)} %get-tuple-element.54), channel_id=1, source_target_pairs={{0,120},{8,0},{16,8},{24,16},{32,24},{40,32},{48,40},{56,48},{64,5... | collective-permute-start | bytes 393224 | tf_op jit(solution)/shard_map/ppermute | solution.py:475
  155.5 11.9 %collective-permute-start.31 = (bf16[128,256]{1,0:T(8,128)(2,1)S(1)}, bf16[128,256]{1,0:T(8,128)(2,1)S(1)}, u32[]{:S(2)}, u32[]{:S(2)}) collective-permute-start(bf16[128,256]{1,0:T(8,128)(2,1)S(1)} %get-tuple-element.84), channel_id=1, source_target_pairs={{0,32},{8,40},{16,48},{24,56},{32,0},{40,8},{48,16},{56,24},{64,96... | collective-permute-start | bytes 196616 | tf_op jit(solution)/shard_map/ppermute | solution.py:480
  159.6 9.3 %collective-permute-start.33 = (bf16[128,256]{1,0:T(8,128)(2,1)S(1)}, bf16[128,256]{1,0:T(8,128)(2,1)S(1)}, u32[]{:S(2)}, u32[]{:S(2)}) collective-permute-start(bf16[128,256]{1,0:T(8,128)(2,1)S(1)} %get-tuple-element.85), channel_id=1, source_target_pairs={{0,96},{8,104},{16,112},{24,120},{32,64},{40,72},{48,80},{56,88},{... | collective-permute-start | bytes 196616 | tf_op jit(solution)/shard_map/ppermute | solution.py:480
  169.0 9.3 %collective-permute-start.32 = (bf16[128,256]{1,0:T(8,128)(2,1)S(1)}, bf16[128,256]{1,0:T(8,128)(2,1)S(1)}, u32[]{:S(2)}, u32[]{:S(2)}) collective-permute-start(bf16[128,256]{1,0:T(8,128)(2,1)S(1)} %get-tuple-element.82), channel_id=1, source_target_pairs={{0,96},{8,104},{16,112},{24,120},{32,64},{40,72},{48,80},{56,88},{... | collective-permute-start | bytes 196616 | tf_op jit(solution)/shard_map/ppermute | solution.py:480
  173.9 10.5 %collective-permute-start.34 = (bf16[128,256]{1,0:T(8,128)(2,1)S(1)}, bf16[128,256]{1,0:T(8,128)(2,1)S(1)}, u32[]{:S(2)}, u32[]{:S(2)}) collective-permute-start(bf16[128,256]{1,0:T(8,128)(2,1)S(1)} %get-tuple-element.83), channel_id=1, source_target_pairs={{0,32},{8,40},{16,48},{24,56},{32,0},{40,8},{48,16},{56,24},{64,96... | collective-permute-start | bytes 196616 | tf_op jit(solution)/shard_map/ppermute | solution.py:480
  184.4 8.0 %collective-permute-start.37 = (bf16[128,512]{1,0:T(8,128)(2,1)S(1)}, bf16[128,512]{1,0:T(8,128)(2,1)S(1)}, u32[]{:S(2)}, u32[]{:S(2)}) collective-permute-start(bf16[128,512]{1,0:T(8,128)(2,1)S(1)} %fusion.1.refs_0_), channel_id=1, source_target_pairs={{0,112},{8,120},{16,0},{24,8},{32,16},{40,24},{48,32},{56,40},{64,... | collective-permute-start | bytes 393224 | tf_op jit(solution)/shard_map/ppermute | solution.py:475
  186.4 6.2 %collective-permute-start.36 = (bf16[128,512]{1,0:T(8,128)(2,1)S(1)}, bf16[128,512]{1,0:T(8,128)(2,1)S(1)}, u32[]{:S(2)}, u32[]{:S(2)}) collective-permute-start(bf16[128,512]{1,0:T(8,128)(2,1)S(1)} %fusion.1.refs_0_), channel_id=1, source_target_pairs={{0,8},{8,16},{16,24},{24,32},{32,40},{40,48},{48,56},{56,64},{64,7... | collective-permute-start | bytes 393224 | tf_op jit(solution)/shard_map/ppermute | solution.py:475
  188.6 8.0 %collective-permute-start.35 = (bf16[128,512]{1,0:T(8,128)(2,1)S(1)}, bf16[128,512]{1,0:T(8,128)(2,1)S(1)}, u32[]{:S(2)}, u32[]{:S(2)}) collective-permute-start(bf16[128,512]{1,0:T(8,128)(2,1)S(1)} %fusion.1.refs_0_), channel_id=1, source_target_pairs={{0,120},{8,0},{16,8},{24,16},{32,24},{40,32},{48,40},{56,48},{64,5... | collective-permute-start | bytes 393224 | tf_op jit(solution)/shard_map/ppermute | solution.py:475
